TPU v7x, 128 devices: a whole 4x4x4 slice. The times are simulated.
128 devices in a mesh: st: 64 (over z, y, x), tp: 2 (over core).
Axes of the slice: x: 4, y: 4, z: 4, core: 2. Of those that a mesh axis runs over, the one named last changes fastest.
Arguments:
- tokens: bfloat16 [65536, 2048], P('st', 'tp'), may hold values from -6 to 6
- norm_gain: float32 [2048], replicated, may hold values from 0.1 to 1.9
- branch_outer: bfloat16 [2048, 2048], P(None, 'tp'), may hold values from -0.125 to 0.125
- branch_gate: bfloat16 [2048, 2048], P(None, 'tp'), may hold values from -0.125 to 0.125
- branch_input: bfloat16 [2048, 2048], P(None, 'tp'), may hold values from -0.125 to 0.125
- conv_taps: float32 [3, 2048], P(None, 'tp'), may hold values from -3.5 to 3.5
- query_weight: bfloat16 [2048, 1024], P(None, 'tp'), may hold values from -0.125 to 0.125
- query_gain: float32 [128], replicated, may hold values from 0.1 to 1.9
- head_scale: float32 [8], P('tp'), may hold values from 1 to 240
- store: bfloat16 [1024, 64, 2048], P('st'), may hold values from -6 to 6
- store_gain: float32 [2048], replicated, may hold values from 0.1 to 1.9
- key_weight: bfloat16 [2048, 256], P(None, 'tp'), may hold values from -0.125 to 0.125
- value_weight: bfloat16 [2048, 256], P(None, 'tp'), may hold values from -0.125 to 0.125
- key_gain: float32 [128], replicated, may hold values from 0.1 to 1.9
- out_weight: bfloat16 [1024, 2048], P(None, 'tp'), may hold values from -0.1875 to 0.1875
- gate_logit: float32 [2048], P('tp'), may hold values from -1 to 4
- passage_ids: int32 [1024, 4], P('st'), may hold values from 0 to 1023, as said below
Outputs:
- mixed: bfloat16 [65536, 2048], P('st', 'tp')
Inputs may be any that keep to these rules, and one draw needn't show every extreme that they name: `passage_ids`: passage p lies in the rows of store held by index p // 16 of st. Among the ids of the rows of one device (its 16 blocks), at most 2 name passages held by any one device, and exactly 2 name passages of some one device; each device names a passage of the device before it and one of the device half the axis away.
All inputs are finite; a program needn't handle non-finite values.
Results may differ from a plain program's by a relative error of at most 0.006.
The roundings to bfloat16 on the way count: a program that leaves them out, or rounds other values in their place, can miss the bound.
Values may be sent and summed in bfloat16 or wider, within the bound.
A program may use at most 128 MiB of HBM per device.

v0:
```python
import math

import jax
import jax.numpy as jnp
from jax import lax
from jax.sharding import PartitionSpec as P

SEQ = 128


EPS = 1e-06


def norm_rows(values, gain):
    values = values.astype(jnp.float32)
    return values * lax.rsqrt(jnp.mean(values * values, axis=-1, keepdims=True) + EPS) * gain


def causal_taps(product, conv_taps):
    token_rows, model_width = product.shape
    grouped = product.reshape(token_rows // SEQ, SEQ, model_width)
    padded = jnp.pad(grouped, ((0, 0), (2, 0), (0, 0)))
    summed = (
        padded[:, 0:SEQ] * conv_taps[0]
        + padded[:, 1 : SEQ + 1] * conv_taps[1]
        + padded[:, 2 : SEQ + 2] * conv_taps[2]
    )
    return summed.reshape(token_rows, model_width)


def passage_partials(queries, key_rows, value_rows):
    scores = jnp.einsum("nqgrd,nkgd->ngrqk", queries, key_rows, preferred_element_type=jnp.float32)
    maxima = jnp.max(scores, axis=-1)
    weights = jnp.exp(scores - maxima[..., None])
    totals = jnp.sum(weights, axis=-1)
    shares = (weights / totals[..., None]).astype(jnp.bfloat16)
    partial_value = jnp.einsum(
        "ngrqk,nkgd->nqgrd", shares, value_rows, preferred_element_type=jnp.float32
    ).astype(jnp.bfloat16)
    return (partial_value, maxima, totals)


def combine_passages(partial_value, maxima, totals):
    highest = jnp.max(maxima, axis=1, keepdims=True)
    weight = jnp.exp(maxima - highest) * totals
    denominator = jnp.sum(weight, axis=1)
    weight = jnp.transpose(weight, (0, 1, 4, 2, 3))
    summed = jnp.sum(partial_value.astype(jnp.float32) * weight[..., None], axis=1)
    return summed / jnp.transpose(denominator, (0, 3, 1, 2))[..., None]


def on_device(
    tokens,
    norm_gain,
    branch_outer,
    branch_gate,
    branch_input,
    conv_taps,
    query_weight,
    query_gain,
    head_scale,
    store,
    store_gain,
    key_weight,
    value_weight,
    key_gain,
    out_weight,
    gate_logit,
    passage_ids,
):
    whole = lax.all_gather(tokens, "tp", axis=1, tiled=True)
    normed = norm_rows(whole, norm_gain).astype(jnp.bfloat16)
    gate_outer = jnp.dot(normed, branch_outer, preferred_element_type=jnp.float32)
    gate_inner = jnp.dot(normed, branch_gate, preferred_element_type=jnp.float32)
    conv_input = jnp.dot(normed, branch_input, preferred_element_type=jnp.float32)
    conv_out = gate_outer * causal_taps(gate_inner * conv_input, conv_taps)
    token_rows = whole.shape[0]
    head_dim = query_gain.shape[0]
    local_heads = query_weight.shape[1] // head_dim
    local_groups = key_weight.shape[1] // head_dim
    repeat = local_heads // local_groups
    block_count, per_block = passage_ids.shape
    block_rows = token_rows // block_count
    raw_query = jnp.dot(normed, query_weight, preferred_element_type=jnp.float32).reshape(
        token_rows, local_heads, head_dim
    )
    queries = (
        norm_rows(raw_query, query_gain) * (head_scale[:, None] / math.sqrt(head_dim))
    ).astype(jnp.bfloat16)
    queries = queries.reshape(block_count, block_rows, local_groups, repeat, head_dim)
    passages_here, passage_rows, model_width = store.shape
    memory = norm_rows(store.reshape(passages_here * passage_rows, model_width), store_gain).astype(
        jnp.bfloat16
    )
    raw_key = jnp.dot(memory, key_weight, preferred_element_type=jnp.float32).reshape(
        passages_here * passage_rows, local_groups, head_dim
    )
    key_rows = (
        norm_rows(raw_key, key_gain)
        .astype(jnp.bfloat16)
        .reshape(passages_here, passage_rows, local_groups * head_dim)
    )
    value_rows = jnp.dot(memory, value_weight, preferred_element_type=jnp.float32).astype(
        jnp.bfloat16
    )
    value_rows = value_rows.reshape(passages_here, passage_rows, local_groups * head_dim)
    pair_table = jnp.concatenate([key_rows, value_rows], axis=2)
    devices = lax.axis_size("st")
    requests = block_count * per_block
    capacity = max(2, (requests + devices - 1) // devices)
    flat_ids = passage_ids.reshape(requests)
    owners = flat_ids // passages_here
    local_index = flat_ids - owners * passages_here
    request_order = jnp.arange(requests, dtype=jnp.int32)
    same_owner = (owners[:, None] == owners[None, :]) & (
        request_order[None, :] < request_order[:, None]
    )
    slot_rank = jnp.sum(same_owner.astype(jnp.int32), axis=1)
    slot_index = owners * capacity + slot_rank
    slot_match = slot_index[:, None] == jnp.arange(devices * capacity, dtype=jnp.int32)[None, :]
    asked = (jnp.sum(jnp.where(slot_match, local_index[:, None] + 1, 0), axis=0) - 1).reshape(
        devices, capacity
    )
    picked = jnp.clip(
        lax.all_to_all(asked, "st", split_axis=0, concat_axis=0, tiled=True), 0, passages_here - 1
    )
    fetched = lax.all_to_all(
        jnp.take(pair_table, picked, axis=0), "st", split_axis=0, concat_axis=0, tiled=True
    )
    received = jnp.take(fetched.reshape(devices * capacity, passage_rows, -1), slot_index, axis=0)
    received = received.reshape(requests, passage_rows, 2, local_groups, head_dim)
    asked_query = jnp.broadcast_to(queries[:, None], (block_count, per_block) + queries.shape[1:])
    asked_query = asked_query.reshape((requests,) + queries.shape[1:])
    partial_value, maxima, totals = passage_partials(
        asked_query, received[:, :, 0], received[:, :, 1]
    )
    partial_value = partial_value.reshape(
        block_count, per_block, block_rows, local_groups, repeat, head_dim
    )
    maxima = maxima.reshape(block_count, per_block, local_groups, repeat, block_rows)
    totals = totals.reshape(block_count, per_block, local_groups, repeat, block_rows)
    attended = (
        combine_passages(partial_value, maxima, totals)
        .astype(jnp.bfloat16)
        .reshape(token_rows, local_heads * head_dim)
    )
    cross = jnp.dot(
        lax.all_gather(attended, "tp", axis=1, tiled=True),
        out_weight,
        preferred_element_type=jnp.float32,
    )
    mixed = conv_out + jax.nn.sigmoid(gate_logit) * cross
    return mixed.astype(jnp.bfloat16)


def solution(mesh):
    return jax.shard_map(
        on_device,
        mesh=mesh,
        in_specs=(
            P("st", "tp"),
            P(),
            P(None, "tp"),
            P(None, "tp"),
            P(None, "tp"),
            P(None, "tp"),
            P(None, "tp"),
            P(),
            P("tp"),
            P("st", None, None),
            P(),
            P(None, "tp"),
            P(None, "tp"),
            P(),
            P(None, "tp"),
            P("tp"),
            P("st", None),
        ),
        out_specs=P("st", "tp"),
        check_vma=False,
    )
```

profile of v0, /device:TPU:1, one launch (start us, length us, event | category | flops | bytes accessed | tf_op | source)
XLA Modules:
  0.0 181.8 jit_solution(10363115677365429428)
XLA Ops:
  8.6 12.0 %all-to-all-start = ((s32[64,1,2]{2,1,0:T(1,128)}), s32[64,1,2]{2,1,0:T(1,128)S(1)}, u32[]{:S(2)}, u32[]{:S(2)}) async-start(s32[64,1,2]{2,1,0:T(1,128)} %bitcast.5), calls=%async_computation | async-start | bytes 65536 | tf_op jit(solution)/shard_map/all_to_all | solution.py:125
  20.6 3.1 %multiply_reduce_fusion.1 = f32[16,64]{1,0:T(8,128)S(1)} fusion(bf16[16,64,2048]{2,1,0:T(8,128)(2,1)} %param.26), kind=kLoop, calls=%fused_computation.15 | loop fusion | flops 6290432 | bytes 4198400 | tf_op jit(solution)/shard_map/reduce_sum | solution.py:16
  23.8 3.3 %fusion.5 = bf16[1024,2048]{1,0:T(8,128)(2,1)S(1)} fusion(f32[2048]{0:T(1024)S(1)} %copy-done.5, f32[1024]{0:T(1024)S(1)} %rsqrt.40, bf16[16,64,2048]{2,1,0:T(8,128)(2,1)} %param.26), kind=kLoop, calls=%fused_computation.12 | loop fusion | flops 8388608 | bytes 8400896 | tf_op jit(solution)/shard_map/convert_element_type | solution.py:92
  30.5 2.7 %gather_fusion = bf16[128,64,256]{2,1,0:T(8,128)(2,1)} fusion(bf16[16,64,256]{2,1,0:T(8,128)(2,1)S(1)} %pad_maximum_fusion, s32[1024]{0:T(1024)S(1)} %pad_clamp_fusion.1), kind=kCustom, calls=%fused_computation | custom fusion | bytes 8389120 | tf_op jit(solution)/shard_map/jit(_take)/gather | solution.py:128
  33.2 4.6 %broadcast_select_fusion = bf16[64,2,64,256]{3,2,1,0:T(8,128)(2,1)} fusion(bf16[64,2,64,256]{3,2,1,0:T(8,128)(2,1)} %bitcast.111, pred[64,2]{1,0:T(8,128)(4,1)S(1)} %copy.77), kind=kLoop, calls=%fused_computation.30 | loop fusion | flops 2097152 | bytes 8388736 | tf_op jit(solution)/shard_map/jit(_take)/select_n | solution.py:128
  37.8 10.2 %all-to-all-start.1 = ((bf16[64,2,64,256]{3,2,1,0:T(8,128)(2,1)}), bf16[64,2,64,256]{3,2,1,0:T(8,128)(2,1)}, u32[]{:S(2)}, u32[]{:S(2)}) async-start(bf16[64,2,64,256]{3,2,1,0:T(8,128)(2,1)} %broadcast_select_fusion), calls=%async_computation.1 | async-start | bytes 8388608 | tf_op jit(solution)/shard_map/all_to_all | solution.py:127
  49.1 49.7 %all-to-all-done.1 = bf16[64,2,64,256]{3,2,1,0:T(8,128)(2,1)} async-done(((bf16[64,2,64,256]{3,2,1,0:T(8,128)(2,1)}), bf16[64,2,64,256]{3,2,1,0:T(8,128)(2,1)}, u32[]{:S(2)}, u32[]{:S(2)}) %all-to-all-start.1) | async-done | bytes 4194336 | tf_op jit(solution)/shard_map/all_to_all | solution.py:127
  98.9 4.2 %gather_fusion.1 = bf16[64,64,256]{2,1,0:T(8,128)(2,1)} fusion(bf16[128,64,256]{2,1,0:T(8,128)(2,1)} %bitcast.12, s32[1024]{0:T(1024)S(1)} %pad_clamp_fusion), kind=kCustom, calls=%fused_computation.1 | custom fusion | bytes 4194560 | tf_op jit(solution)/shard_map/jit(_take)/gather | solution.py:130
  103.0 4.0 %gather.12 = bf16[64,64,2,1,128]{4,2,1,0,3:T(2,128)(2,1)} reshape(bf16[64,64,256]{2,1,0:T(8,128)(2,1)} %gather_fusion.1) | data formatting | bytes 4194304 | tf_op jit(solution)/shard_map/jit(_take)/gather | solution.py:130
  107.0 3.3 %copy_select_fusion = bf16[64,64,2,1,128]{4,1,0,3,2:T(8,128)(2,1)} fusion(bf16[64,64,2,1,128]{4,2,1,0,3:T(2,128)(2,1)} %gather.12, pred[64]{0:T(512)(128)(4,1)S(1)} %get-tuple-element.5), kind=kLoop, calls=%fused_computation.33 | loop fusion | flops 1048576 | bytes 4194368 | tf_op jit(solution)/shard_map/jit(_take)/select_n | solution.py:130
  110.3 3.2 %fusion = f32[1024]{0:T(1024)S(1)} fusion(bf16[1024,2048]{1,0:T(8,128)(2,1)} %all-gather.3.cloned.1.call-done), kind=kLoop, calls=%fused_computation.4 | loop fusion | flops 6290432 | bytes 4198400 | tf_op jit(solution)/shard_map/reduce_sum | solution.py:16
  113.7 5.5 %bitcast_reduce_fusion.1 = (f32[1024,4]{0,1:T(4,128)S(1)}, f32[1024,512]{0,1:T(8,128)}) fusion(bf16[2048,512]{1,0:T(8,128)(2,1)} %param.23, bf16[1024,2048]{1,0:T(8,128)(2,1)S(1)} %copy-done.2, f32[2048]{0:T(1024)S(1)} %copy-done.13, f32[1024]{0:T(1024)S(1)} %add_rsqrt_fusion.3), kind=kOutput, calls=%fused_computation.32 | convolution fusion | flops 2156916736 | bytes 8417280 | tf_op jit(solution)/shard_map/dot_general | solution.py:84
  119.3 2.9 %copy.81 = f32[1024,512]{1,0:T(8,128)} copy(f32[1024,512]{0,1:T(8,128)} %get-tuple-element.15) | data formatting | bytes 4194304 | tf_op jit(solution)/shard_map/dot_general | solution.py:84
  122.2 2.9 %reshape.452 = f32[16,64,4,128]{3,2,1,0:T(4,128)} reshape(f32[1024,512]{1,0:T(8,128)} %copy.81) | data formatting | bytes 4194304 | tf_op jit(solution)/shard_map/reshape | solution.py:84
  125.3 3.4 %multiply_convert_fusion = bf16[16,64,4,128]{3,2,1,0:T(4,128)(2,1)S(1)} fusion(f32[16,64,4,128]{3,2,1,0:T(4,128)} %reshape.452, f32[4]{0:T(128)S(1)} %broadcast_multiply_fusion, f32[128]{0:T(128)S(1)} %copy-done.7, f32[16,64,4]{2,1,0:T(8,128)S(1)} %bitcast.118), kind=kLoop, calls=%fused_computation.35 | loop fusion | flops 2097152 | bytes 3162640 | tf_op jit(solution)/shard_map/convert_element_type | solution.py:89
  130.3 4.3 %bitcast_reduce_fusion = (f32[64,4,64]{2,1,0:T(4,128)S(1)}, f32[64,64,64,4]{2,1,3,0:T(8,128)S(1)}) fusion(bf16[64,64,4,128]{3,1,2,0:T(8,128)(2,1)S(1)} %bitcast.112, bf16[64,64,2,1,128]{4,1,0,3,2:T(8,128)(2,1)S(1)} %copy-done.1), kind=kOutput, calls=%fused_computation.8 | convolution fusion | flops 269467648 | bytes 9502720 | tf_op jit(solution)/shard_map/nqgrd,nkgd->ngrqk/dot_general | solution.py:32
  134.7 2.5 %fusion.6 = f32[64,4,64]{2,1,0:T(4,128)S(1)} fusion(f32[64,64,64,4]{2,1,3,0:T(8,128)S(1)} %get-tuple-element.19, f32[64,4,64]{2,1,0:T(4,128)S(1)} %get-tuple-element.18), kind=kLoop, calls=%fused_computation.16 | loop fusion | flops 2080768 | bytes 4325376 | tf_op jit(solution)/shard_map/reduce_sum | solution.py:35
  137.1 1.8 bitcast_convert_fusion
  139.0 2.6 %multiply_reduce_fusion = f32[16,64,4,128]{3,1,2,0:T(8,128)S(1)} fusion(f32[16,4,64,1,4,128]{5,2,4,1,0,3:T(8,128)S(1)} %bitcast.113, f32[16,4,64,4]{2,3,1,0:T(4,128)S(1)} %get-tuple-element.10), kind=kLoop, calls=%fused_computation.13 | loop fusion | flops 3670016 | bytes 10551296 | tf_op jit(solution)/shard_map/reduce_sum | solution.py:48
  144.5 8.3 %fusion.26 = f32[1024,1024]{1,0:T(8,128)S(1)} fusion(bf16[2048,1024]{1,0:T(8,128)(2,1)} %param.20, bf16[1024,2048]{1,0:T(8,128)(2,1)} %all-gather.3.cloned.1.call-done, f32[2048]{0:T(1024)S(1)} %copy-done.13, f32[1024]{0:T(1024)S(1)} %add_rsqrt_fusion.3), kind=kOutput, calls=%fused_computation.81 | convolution fusion | flops 4303355904 | bytes 12595200 | tf_op jit(solution)/shard_map/dot_general | solution.py:74
  152.8 4.6 %convolution_multiply_fusion = f32[1024,1024]{1,0:T(8,128)S(1)} fusion(f32[1024,1024]{1,0:T(8,128)S(1)} %fusion.26, bf16[2048,1024]{1,0:T(8,128)(2,1)S(1)} %copy-done.9, bf16[1024,2048]{1,0:T(8,128)(2,1)S(1)} %copy-done.3, f32[2048]{0:T(1024)S(1)} %copy-done.13, f32[1024]{0:T(1024)S(1)} %add_rsqrt_fusion.3), kind=kOutput, calls=%fused_computation.31 | convolution fusion | flops 4304404480 | bytes 16789504 | tf_op jit(solution)/shard_map/dot_general | solution.py:75
  157.5 3.2 %fusion.9 = f32[8,128,1024]{2,1,0:T(8,128)} fusion(f32[8,128,1024]{2,1,0:T(8,128)S(1)} %bitcast.114, f32[1024]{0:T(1024)S(1)} %bitcast.124, f32[1024]{0:T(1024)S(1)} %bitcast.125, f32[1024]{0:T(1024)S(1)} %bitcast.123), kind=kLoop, calls=%fused_computation.21 | loop fusion | flops 5242880 | bytes 8400896 | tf_op jit(solution)/shard_map/add | solution.py:24
  161.0 6.3 %fusion.28 = f32[1024,1024]{1,0:T(8,128)} fusion(bf16[2048,1024]{1,0:T(8,128)(2,1)S(1)} %copy-done.10, bf16[1024,2048]{1,0:T(8,128)(2,1)S(1)} %copy-done.3, f32[2048]{0:T(1024)S(1)} %copy-done.13, f32[1024]{0:T(1024)S(1)} %add_rsqrt_fusion.3), kind=kOutput, calls=%fused_computation.82 | convolution fusion | flops 4303355904 | bytes 12595200 | tf_op jit(solution)/shard_map/dot_general | solution.py:73
  167.3 7.7 %fusion.14 = bf16[1024,1024]{1,0:T(8,128)(2,1)} fusion(f32[1024,1024]{1,0:T(8,128)} %fusion.28, f32[8,128,1024]{2,1,0:T(8,128)} %fusion.9, bf16[1024,1024]{1,0:T(8,128)(2,1)} %all-gather.5.cloned.1.call-done, bf16[1024,1024]{1,0:T(8,128)(2,1)S(1)} %copy-done, f32[1024]{0:T(1024)S(1)} %add_divide_fusion), kind=kOutput, calls=%fused_computation.28 | convolution fusion | flops 2151677952 | bytes 14684160 | tf_op jit(solution)/shard_map/dot_general | solution.py:147
  (75 shorter events, 11.9 us)
Async XLA Ops:
  6.5 160.7 %copy-start = (bf16[1024,1024]{1,0:T(8,128)(2,1)S(1)}, bf16[1024,1024]{1,0:T(8,128)(2,1)}, u32[]{:S(2)}) copy-start(bf16[1024,1024]{1,0:T(8,128)(2,1)} %param.31) | copy-start | bytes 6291460
  6.5 17.2 %copy-start.5 = (f32[2048]{0:T(1024)S(1)}, f32[2048]{0:T(1024)}, u32[]{:S(2)}) copy-start(f32[2048]{0:T(1024)} %param.27) | copy-start | bytes 24580
  8.6 21.4 %all-to-all-start = ((s32[64,1,2]{2,1,0:T(1,128)}), s32[64,1,2]{2,1,0:T(1,128)S(1)}, u32[]{:S(2)}, u32[]{:S(2)}) async-start(s32[64,1,2]{2,1,0:T(1,128)} %bitcast.5), calls=%async_computation | async-start | bytes 65536 | tf_op jit(solution)/shard_map/all_to_all | solution.py:125
  23.8 3.3 %copy-start.11 = (bf16[2048,128]{1,0:T(8,128)(2,1)S(1)}, bf16[2048,128]{1,0:T(8,128)(2,1)}, u32[]{:S(2)}) copy-start(bf16[2048,128]{1,0:T(8,128)(2,1)} %param.28) | copy-start | bytes 1572868
  27.1 1.4 copy-start.12
  28.4 1.3 copy-start.8
  37.8 11.3 %copy-start.14 = (f32[4]{0:T(128)S(1)}, f32[4]{0:T(128)}, u32[]{:S(2)}) copy-start(f32[4]{0:T(128)} %param.25) | copy-start | bytes 52
  37.8 11.3 %copy-start.6 = (f32[1024]{0:T(1024)S(1)}, f32[1024]{0:T(1024)}, u32[]{:S(2)}) copy-start(f32[1024]{0:T(1024)} %param.32) | copy-start | bytes 12292
  37.8 11.3 %copy-start.4 = (f32[3,1024]{1,0:T(4,128)S(1)}, f32[3,1024]{1,0:T(4,128)}, u32[]{:S(2)}) copy-start(f32[3,1024]{1,0:T(4,128)} %param.22) | copy-start | bytes 36868
  37.8 61.0 %all-to-all-start.1 = ((bf16[64,2,64,256]{3,2,1,0:T(8,128)(2,1)}), bf16[64,2,64,256]{3,2,1,0:T(8,128)(2,1)}, u32[]{:S(2)}, u32[]{:S(2)}) async-start(bf16[64,2,64,256]{3,2,1,0:T(8,128)(2,1)} %broadcast_select_fusion), calls=%async_computation.1 | async-start | bytes 8388608 | tf_op jit(solution)/shard_map/all_to_all | solution.py:127
  48.0 62.3 %all-gather.3.cloned.1.call-start = ((), (), s32[]{:S(2)}) async-start(), calls=%async_computation.2 | async-start | bytes 6291456 | tf_op jit(solution)/shard_map/all_gather | solution.py:71
  48.7 118.5 %all-gather.5.cloned.1.call-start = ((), (), s32[]{:S(2)}) async-start(), calls=%async_computation.3 | async-start | bytes 3145728 | tf_op jit(solution)/shard_map/all_gather | solution.py:148
  107.0 6.5 %copy-start.13 = (f32[2048]{0:T(1024)S(1)}, f32[2048]{0:T(1024)}, u32[]{:S(2)}) copy-start(f32[2048]{0:T(1024)} %param.18) | copy-start | bytes 24580
  110.3 3.4 %copy-start.2 = (bf16[1024,2048]{1,0:T(8,128)(2,1)S(1)}, bf16[1024,2048]{1,0:T(8,128)(2,1)}, u32[]{:S(2)}) copy-start(bf16[1024,2048]{1,0:T(8,128)(2,1)} %all-gather.3.cloned.1.call-done) | copy-start | bytes 12582916
  119.3 6.1 %copy-start.7 = (f32[128]{0:T(128)S(1)}, f32[128]{0:T(128)}, u32[]{:S(2)}) copy-start(f32[128]{0:T(128)} %param.24) | copy-start | bytes 1540
  128.7 1.6 copy-start.1
  144.5 8.3 %copy-start.3 = (bf16[1024,2048]{1,0:T(8,128)(2,1)S(1)}, bf16[1024,2048]{1,0:T(8,128)(2,1)}, u32[]{:S(2)}) copy-start(bf16[1024,2048]{1,0:T(8,128)(2,1)} %all-gather.3.cloned.1.call-done) | copy-start | bytes 12582916
  144.5 8.3 %copy-start.9 = (bf16[2048,1024]{1,0:T(8,128)(2,1)S(1)}, bf16[2048,1024]{1,0:T(8,128)(2,1)}, u32[]{:S(2)}) copy-start(bf16[2048,1024]{1,0:T(8,128)(2,1)} %param.21) | copy-start | bytes 12582916
  157.4 3.5 %copy-start.10 = (bf16[2048,1024]{1,0:T(8,128)(2,1)S(1)}, bf16[2048,1024]{1,0:T(8,128)(2,1)}, u32[]{:S(2)}) copy-start(bf16[2048,1024]{1,0:T(8,128)(2,1)} %param.19) | copy-start | bytes 12582916
Sparse Core Ops, SparseCore 0:
  50.5 18.8 all-gather.2
  144.6 15.9 all-gather.4
where the time goes:
time: 184 us; the launch traced here: 182 us
  waiting for transfers between devices  50.4 us (27%)
  matrix products  41.1 us (22%)
  other arithmetic  30.7 us (17%)
  local copies, waits for them, and re-layouts  23.5 us (13%)
  starting transfers between devices  22.4 us (12%)
  between operations  13.8 us (8%)
    all_to_all x1, waiting for transfers between devices, on_device(): lax.all_to_all(jnp.take(pair_table, picked, axis=0), 'st', split_axis=0,...  49.7 us
    all_to_all x1, starting transfers between devices, on_device(): lax.all_to_all(asked, 'st', split_axis=0, concat_axis=0, tiled=True)  12 us
    all_to_all x1, starting transfers between devices, on_device(): lax.all_to_all(jnp.take(pair_table, picked, axis=0), 'st', split_axis=0,...  10.2 us
    dot_general x1, matrix products, on_device(): jnp.dot(normed, branch_gate, preferred_element_type=jnp.float32)  8.29 us
    gather x2, local copies, waits for them, and re-layouts, on_device(): jnp.take(fetched.reshape(devices * capacity, passage_rows, -1), slot_inde...  8.17 us
    dot_general x1, matrix products, on_device(): jnp.dot(lax.all_gather(attended, 'tp', axis=1, tiled=True), out_weight, p...  7.74 us
    reduce_sum x2, other arithmetic, norm_rows(): jnp.mean(values * values, axis=-1, keepdims=True) + EPS  6.3 us
    dot_general x1, matrix products, on_device(): jnp.dot(normed, branch_outer, preferred_element_type=jnp.float32)  6.28 us
  transfers between devices with their start and end apart: 4, of which 1 were waited for; matrix products, arithmetic and copies ran while one was open for 24% of the time, Pallas kernels for 0%

commit v1 on v0

v1 whole, which is shorter than its diff:
```python
import math

import jax
import jax.numpy as jnp
from jax import lax
from jax.experimental import pallas as pl
from jax.experimental.pallas import tpu as pltpu
from jax.sharding import PartitionSpec as P

MESH = pl.DeviceIdType.MESH
EPS = 1e-06
SEQ = 128
RING = 4
CAP = 2
HD = 128
PLEN = 64
BF = jnp.bfloat16
F32 = jnp.float32

ORDERS = (("z", "y", "x"), ("y", "x", "z"), ("x", "z", "y"))
ROWS = (48, 48, 32)
STRIDE = {"z": RING * RING, "y": RING, "x": 1}
GROUP = ((0,), (1, 2, 3))
OFFS = (1, 3, 2)


def coordinates(st):
    return {"z": st // 16, "y": lax.rem(st // 4, 4), "x": lax.rem(st, 4)}


def shifted(st, moves):
    at = coordinates(st)
    out = 0
    for axis in ("z", "y", "x"):
        out = out + lax.rem(at[axis] + (moves.get(axis, 0) % RING), RING) * STRIDE[axis]
    return out


def position(group, oc, ob):
    return (oc * RING + ob) * CAP if group == 0 else RING * RING * CAP + (oc * RING + ob) * 3 * CAP


PLANE = [
    (z, y, x)
    for z in range(RING)
    for y in range(RING)
    for x in range(RING)
    if (z, y, x) != (0, 0, 0) and min(z, y, x) == 0
]


def rel_index(moves):
    return (moves.get("z", 0) * RING + moves.get("y", 0)) * RING + moves.get("x", 0)


def kernel(
    slots,
    tokens,
    norm_gain,
    w_outer,
    w_gate,
    w_input,
    taps,
    w_query,
    query_gain,
    head_scale,
    store,
    store_gain,
    w_key,
    w_value,
    key_gain,
    w_out,
    gate_logit,
    asked,
    out,
    v_store,
    v_wkv,
    v_mem,
    v_x,
    v_n,
    v_wo,
    v_wg,
    v_wi,
    v_wq,
    v_wout,
    v_q,
    v_conv,
    v_att,
    v_attp,
    v_out,
    v_ask,
    s_ask,
    v_k,
    v_v,
    *rest,
):
    table = [rest[f * 4 : f * 4 + 4] for f in range(3)]
    rest = rest[12:]
    packed = [rest[f * 2 : f * 2 + 2] for f in range(3)]
    rest = rest[6:]
    relay = [rest[f * 2 : f * 2 + 2] for f in range(3)]
    rest = rest[6:]
    final = rest[:3]
    (
        local_sem,
        store_sem,
        out_sem,
        ask_ss,
        ask_rs,
        tok_ss,
        tok_rs,
        a_ss,
        a_rs,
        b_ss,
        b_rs,
        c_ss,
        c_rs,
        att_ss,
        att_rs,
    ) = rest[3:]

    st = lax.axis_index("st")
    tp = lax.axis_index("tp")
    other = 1 - tp
    rows_tok = tokens.shape[0]
    half = tokens.shape[1]
    width = 2 * half
    n_pass = store.shape[0] // PLEN

    store_copies = []
    wk = pltpu.make_async_copy(w_key, v_wkv.at[:, pl.ds(0, HD)], local_sem.at[0])
    wv = pltpu.make_async_copy(w_value, v_wkv.at[:, pl.ds(HD, HD)], local_sem.at[1])
    chunk = 256
    for p in range(4):
        store_copies.append(
            pltpu.make_async_copy(
                store.at[pl.ds(p * chunk, chunk)], v_store.at[pl.ds(p * chunk, chunk)], store_sem.at[p]
            )
        )
    store_copies[0].start()
    wk.start()
    wv.start()
    for p in range(1, 4):
        store_copies[p].start()
    tok_local = pltpu.make_async_copy(tokens, v_x.at[tp], local_sem.at[2])
    tok_local.start()
    weights = []
    for i, (src, dst) in enumerate(
        ((w_query, v_wq), (w_outer, v_wo), (w_gate, v_wg), (w_input, v_wi), (w_out, v_wout))
    ):
        cp = pltpu.make_async_copy(src, dst, local_sem.at[3 + i])
        cp.start()
        weights.append(cp)

    barrier = pltpu.get_barrier_semaphore()
    for z, y, x in PLANE:
        pl.semaphore_signal(
            barrier, inc=1, device_id=(shifted(st, {"z": z, "y": y, "x": x}), tp), device_id_type=MESH
        )
    pl.semaphore_signal(barrier, inc=1, device_id=(st, other), device_id_type=MESH)
    pl.semaphore_wait(barrier, len(PLANE) + 1)

    ask_copies = []
    for i, (z, y, x) in enumerate(PLANE):
        cp = pltpu.make_async_remote_copy(
            src_ref=asked,
            dst_ref=v_ask.at[rel_index({"z": z, "y": y, "x": x})],
            send_sem=ask_ss.at[i],
            recv_sem=ask_rs.at[i],
            device_id=(shifted(st, {"z": -z, "y": -y, "x": -x}), tp),
            device_id_type=MESH,
        )
        cp.start()
        ask_copies.append(cp)
    tok_remote = pltpu.make_async_remote_copy(
        src_ref=tokens,
        dst_ref=v_x.at[tp],
        send_sem=tok_ss,
        recv_sem=tok_rs,
        device_id=(st, other),
        device_id_type=MESH,
    )
    tok_remote.start()
    v_ask[0] = asked[...]

    def a_copy(f, o, p):
        return pltpu.make_async_remote_copy(
            src_ref=table[f][0].at[pl.ds(p * 4, 4)],
            dst_ref=table[f][o].at[pl.ds(p * 4, 4)],
            send_sem=a_ss.at[f * 3 + o - 1, p],
            recv_sem=a_rs.at[f * 3 + o - 1, p],
            device_id=(shifted(st, {ORDERS[f][0]: o}), tp),
            device_id_type=MESH,
        )

    wk.wait()
    wv.wait()
    sub = 32

    def kv_chunk(p, carry):
        base = p * chunk
        pltpu.make_async_copy(
            store.at[pl.ds(base, chunk)], v_store.at[pl.ds(base, chunk)], store_sem.at[p]
        ).wait()

        def norm_sub(i, c):
            x = v_store[pl.ds(base + i * sub, sub), :].astype(F32)
            r = lax.rsqrt(jnp.mean(x * x, axis=-1, keepdims=True) + EPS)
            v_mem[pl.ds(i * sub, sub), :] = (x * r * store_gain[...]).astype(BF)
            return c

        lax.fori_loop(0, chunk // sub, norm_sub, 0, unroll=2)
        kv = jnp.dot(v_mem[...], v_wkv[...], preferred_element_type=F32)
        k = kv[:, :HD]
        k = k * lax.rsqrt(jnp.mean(k * k, axis=-1, keepdims=True) + EPS) * key_gain[...]
        k = k.astype(BF).reshape(4, PLEN, HD)
        v = kv[:, HD:].astype(BF).reshape(4, PLEN, HD)
        at = pl.ds(p * 4, 4)
        table[0][0][at, :, :] = k[:, 0:48]
        table[1][0][at, 0:16, :] = k[:, 48:64]
        table[1][0][at, 16:48, :] = v[:, 0:32]
        table[2][0][at, :, :] = v[:, 32:64]
        for o in OFFS:
            for f in range(3):
                a_copy(f, o, p).start()
        return carry

    lax.fori_loop(0, 4, kv_chunk, 0)

    for cp in ask_copies:
        cp.wait_recv()
    ask_local = pltpu.make_async_copy(v_ask, s_ask, local_sem.at[8])
    ask_local.start()
    ask_local.wait()

    def pack(group):
        n = len(GROUP[group]) * CAP
        for f in range(3):
            aa, ab, ac = ORDERS[f]
            owners = [shifted(st, {aa: -o}) for o in GROUP[group]]

            def one(t, carry, f=f, ab=ab, ac=ac, owners=owners):
                ob = t // RING
                oc = lax.rem(t, RING)
                rel = ob * STRIDE[ab] + oc * STRIDE[ac]
                for j, o in enumerate(GROUP[group]):
                    for r in range(CAP):
                        at = s_ask[rel, 0, owners[j] * CAP + r]
                        packed[f][group][ob, oc, j * CAP + r] = table[f][o][at]
                return carry

            lax.fori_loop(0, RING * RING, one, 0, unroll=2)
            final[f][pl.ds(position(group, 0, 0), n)] = packed[f][group][0, 0]

    def b_copies(f, group, ob):
        n = len(GROUP[group]) * CAP
        to = (shifted(st, {ORDERS[f][1]: ob}), tp)
        i = (f * 2 + group) * 3 + ob - 1
        return (
            pltpu.make_async_remote_copy(
                src_ref=packed[f][group].at[ob, pl.ds(1, 3)],
                dst_ref=relay[f][group].at[ob - 1],
                send_sem=b_ss.at[i, 0],
                recv_sem=b_rs.at[i, 0],
                device_id=to,
                device_id_type=MESH,
            ),
            pltpu.make_async_remote_copy(
                src_ref=packed[f][group].at[ob, 0],
                dst_ref=final[f].at[pl.ds(position(group, 0, ob), n)],
                send_sem=b_ss.at[i, 1],
                recv_sem=b_rs.at[i, 1],
                device_id=to,
                device_id_type=MESH,
            ),
        )

    def c_copy(f, group, oc, ob):
        n = len(GROUP[group]) * CAP
        i = ((f * 2 + group) * 3 + oc - 1) * 4 + ob
        src = packed[f][group].at[0, oc] if ob == 0 else relay[f][group].at[ob - 1, oc - 1]
        return pltpu.make_async_remote_copy(
            src_ref=src,
            dst_ref=final[f].at[pl.ds(position(group, oc, ob), n)],
            send_sem=c_ss.at[i],
            recv_sem=c_rs.at[i],
            device_id=(shifted(st, {ORDERS[f][2]: oc}), tp),
            device_id_type=MESH,
        )

    def send_packed(group):
        for f in range(3):
            for ob in OFFS:
                b_copies(f, group, ob)[0].start()
        for f in range(3):
            for ob in OFFS:
                b_copies(f, group, ob)[1].start()
        for f in range(3):
            for oc in OFFS:
                c_copy(f, group, oc, 0).start()

    def forward(group, ob):
        for f in range(3):
            b_copies(f, group, ob)[0].wait_recv()
            for oc in OFFS:
                c_copy(f, group, oc, ob).start()

    pack(0)
    send_packed(0)

    tok_local.wait()
    tok_remote.wait_recv()

    def norm_tok(i, c):
        at = pl.ds(i * sub, sub)
        x0 = v_x[0, at, :].astype(F32)
        x1 = v_x[1, at, :].astype(F32)
        total = jnp.sum(x0 * x0, axis=-1, keepdims=True) + jnp.sum(x1 * x1, axis=-1, keepdims=True)
        r = lax.rsqrt(total * (1.0 / width) + EPS)
        v_n[at, pl.ds(0, half)] = (x0 * r * norm_gain[:, 0:half]).astype(BF)
        v_n[at, pl.ds(half, half)] = (x1 * r * norm_gain[:, half:width]).astype(BF)
        return c

    lax.fori_loop(0, rows_tok // sub, norm_tok, 0, unroll=2)

    weights[0].wait()
    n_heads = v_q.shape[1]

    def query_chunk(i, c):
        raw = jnp.dot(v_n[pl.ds(i * chunk, chunk), :], v_wq[...], preferred_element_type=F32)
        for h in range(n_heads):
            q = raw[:, h * HD : (h + 1) * HD]
            q = q * lax.rsqrt(jnp.mean(q * q, axis=-1, keepdims=True) + EPS) * query_gain[...]
            q = (q * (head_scale[h] / math.sqrt(HD))).astype(BF).reshape(chunk // PLEN, PLEN, HD)
            v_q[pl.ds(i * (chunk // PLEN), chunk // PLEN), h] = q
        return c

    lax.fori_loop(0, rows_tok // chunk, query_chunk, 0)

    for f in range(3):
        for o in OFFS:
            for p in range(4):
                a_copy(f, o, p).wait_recv()
    pack(1)
    send_packed(1)

    for cp in weights[1:4]:
        cp.wait()
    tall, wide = 512, 256
    cols = v_wo.shape[1] // wide

    def branch(s, carry):
        rows = pl.ds(pl.multiple_of((s // cols) * tall, tall), tall)
        at = pl.ds(pl.multiple_of(lax.rem(s, cols) * wide, wide), wide)
        n = v_n[rows, :]
        gate = jnp.dot(n, v_wg[:, at], preferred_element_type=F32)
        z = gate * jnp.dot(n, v_wi[:, at], preferred_element_type=F32)
        row = lax.rem(lax.broadcasted_iota(jnp.int32, (tall, wide), 0), SEQ)
        one = jnp.where(row >= 1, pltpu.roll(z, 1, 0), 0.0)
        two = jnp.where(row >= 2, pltpu.roll(z, 2, 0), 0.0)
        t = taps[:, at]
        conv = two * t[0:1] + one * t[1:2] + z * t[2:3]
        v_conv[rows, at] = conv
        v_conv[rows, at] = (
            jnp.dot(n, v_wo[:, at], preferred_element_type=F32) * v_conv[rows, at]
        )

        @pl.when(s == 0)
        def _():
            forward(0, 1)
            forward(0, 3)

        @pl.when(s == 1)
        def _():
            forward(0, 2)

        @pl.when(s == 4)
        def _():
            forward(1, 1)
            forward(1, 3)

        @pl.when(s == 6)
        def _():
            forward(1, 2)

        return carry

    lax.fori_loop(0, (rows_tok // tall) * cols, branch, 0)

    weights[4].wait()
    for f in range(3):
        for group in range(2):
            for ob in OFFS:
                b_copies(f, group, ob)[1].wait_recv()
            for oc in OFFS:
                for ob in range(RING):
                    c_copy(f, group, oc, ob).wait_recv()

    n_blocks = v_q.shape[0]
    per_block = 4

    def attend(b, carry):
        for j in range(per_block):
            first = final[0][slots[0, b * per_block + j]]
            second = final[1][slots[1, b * per_block + j]]
            third = final[2][slots[2, b * per_block + j]]
            v_k[pl.ds(j * PLEN, 48), :] = first
            v_k[pl.ds(j * PLEN + 48, 16), :] = second[0:16]
            v_v[pl.ds(j * PLEN, 32), :] = second[16:48]
            v_v[pl.ds(j * PLEN + 32, 32), :] = third
        q = v_q[b].reshape(n_heads * PLEN, HD)
        scores = lax.dot_general(
            q, v_k[...], (((1,), (1,)), ((), ())), preferred_element_type=F32
        )
        top = jnp.max(scores, axis=-1, keepdims=True)
        weight = jnp.exp(scores - top)
        total = jnp.sum(weight, axis=-1, keepdims=True)
        share = (weight / total).astype(BF)
        value = jnp.dot(share, v_v[...], preferred_element_type=F32).astype(BF)
        at = pl.ds(b * PLEN, PLEN)
        for h in range(n_heads):
            v_att[at, pl.ds(h * HD, HD)] = value[h * PLEN : (h + 1) * PLEN]
        return carry

    def att_copy(i):
        return pltpu.make_async_remote_copy(
            src_ref=v_att.at[pl.ds(i * chunk, chunk)],
            dst_ref=v_attp.at[pl.ds(i * chunk, chunk)],
            send_sem=att_ss.at[i],
            recv_sem=att_rs.at[i],
            device_id=(st, other),
            device_id_type=MESH,
        )

    n_chunks = rows_tok // chunk

    def attend_chunk(i, carry):
        per = n_blocks // n_chunks
        lax.fori_loop(i * per, (i + 1) * per, attend, 0)
        att_copy(i).start()
        return carry

    lax.fori_loop(0, n_chunks, attend_chunk, 0)

    mine = v_att.shape[1]

    def out_copy(i):
        at = pl.ds(i * chunk, chunk)
        return pltpu.make_async_copy(v_out.at[at], out.at[at], out_sem.at[i])

    def project(i, carry):
        at = pl.ds(pl.multiple_of(i * chunk, chunk), chunk)
        att_copy(i).wait_recv()
        cross = jnp.dot(
            v_att[at, :], v_wout[pl.ds(pl.multiple_of(tp * mine, mine), mine), :], preferred_element_type=F32
        )
        cross = cross + jnp.dot(
            v_attp[at, :],
            v_wout[pl.ds(pl.multiple_of(other * mine, mine), mine), :],
            preferred_element_type=F32,
        )
        v_out[at, :] = (v_conv[at, :] + jax.nn.sigmoid(gate_logit[...]) * cross).astype(BF)
        out_copy(i).start()
        return carry

    lax.fori_loop(0, n_chunks, project, 0)

    for i in range(n_chunks):
        out_copy(i).wait()
        att_copy(i).wait_send()
    for cp in ask_copies:
        cp.wait_send()
    tok_remote.wait_send()
    for f in range(3):
        for o in OFFS:
            for p in range(4):
                a_copy(f, o, p).wait_send()
        for group in range(2):
            for ob in OFFS:
                for cp in b_copies(f, group, ob):
                    cp.wait_send()
            for oc in OFFS:
                for ob in range(RING):
                    c_copy(f, group, oc, ob).wait_send()


def request_tables(passage_ids, n_pass, n_st):
    flat = passage_ids.reshape(-1)
    requests = flat.shape[0]
    owner = flat // n_pass
    local = flat - owner * n_pass
    order = jnp.arange(requests, dtype=jnp.int32)
    same = (owner[:, None] == owner[None, :]) & (order[None, :] < order[:, None])
    rank = jnp.sum(same.astype(jnp.int32), axis=1)
    match = (owner * CAP + rank)[:, None] == jnp.arange(n_st * CAP, dtype=jnp.int32)[None, :]
    asked = jnp.sum(jnp.where(match, local[:, None], 0), axis=0).reshape(1, n_st * CAP)
    me = coordinates(lax.axis_index("st"))
    them = coordinates(owner)
    rows = []
    for order_f in ORDERS:
        oa, ob, oc = [lax.rem(me[axis] - them[axis] + RING, RING) for axis in order_f]
        spot = oc * RING + ob
        near = spot * CAP + rank
        far = RING * RING * CAP + spot * 3 * CAP + (oa - 1) * CAP + rank
        rows.append(jnp.where(oa == 0, near, far))
    return asked.astype(jnp.int32), jnp.stack(rows).astype(jnp.int32)


def on_device(
    tokens,
    norm_gain,
    branch_outer,
    branch_gate,
    branch_input,
    conv_taps,
    query_weight,
    query_gain,
    head_scale,
    store,
    store_gain,
    key_weight,
    value_weight,
    key_gain,
    out_weight,
    gate_logit,
    passage_ids,
):
    n_pass, plen, width = store.shape
    n_tok, half = tokens.shape
    heads = head_scale.shape[0]
    n_st = lax.axis_size("st")
    asked, slots = request_tables(passage_ids, n_pass, n_st)
    blocks = passage_ids.shape[0]

    vmem = pl.BlockSpec(memory_space=pltpu.VMEM)
    smem = pl.BlockSpec(memory_space=pltpu.SMEM)
    hbm = pl.BlockSpec(memory_space=pl.ANY)
    dma = pltpu.SemaphoreType.DMA
    scratch = [
        pltpu.VMEM((n_pass * plen, width), BF),
        pltpu.VMEM((width, 2 * HD), BF),
        pltpu.VMEM((256, width), BF),
        pltpu.VMEM((2, n_tok, half), BF),
        pltpu.VMEM((n_tok, width), BF),
        pltpu.VMEM(branch_outer.shape, BF),
        pltpu.VMEM(branch_gate.shape, BF),
        pltpu.VMEM(branch_input.shape, BF),
        pltpu.VMEM(query_weight.shape, BF),
        pltpu.VMEM(out_weight.shape, BF),
        pltpu.VMEM((blocks, heads, plen, HD), BF),
        pltpu.VMEM((n_tok, half), F32),
        pltpu.VMEM((n_tok, heads * HD), BF),
        pltpu.VMEM((n_tok, heads * HD), BF),
        pltpu.VMEM((n_tok, half), BF),
        pltpu.VMEM((n_st, 1, n_st * CAP), jnp.int32),
        pltpu.SMEM((n_st, 1, n_st * CAP), jnp.int32),
        pltpu.VMEM((4 * plen, HD), BF),
        pltpu.VMEM((4 * plen, HD), BF),
    ]
    for f in range(3):
        scratch += [pltpu.VMEM((n_pass, ROWS[f], HD), BF)] * RING
    for f in range(3):
        scratch += [pltpu.VMEM((RING, RING, len(g) * CAP, ROWS[f], HD), BF) for g in GROUP]
    for f in range(3):
        scratch += [pltpu.VMEM((3, 3, len(g) * CAP, ROWS[f], HD), BF) for g in GROUP]
    for f in range(3):
        scratch += [pltpu.VMEM((n_st * CAP, ROWS[f], HD), BF)]
    scratch += [
        dma((9,)),
        dma((4,)),
        dma((4,)),
        dma((len(PLANE),)),
        dma((len(PLANE),)),
        dma,
        dma,
        dma((9, 4)),
        dma((9, 4)),
        dma((18, 2)),
        dma((18, 2)),
        dma((72,)),
        dma((72,)),
        dma((4,)),
        dma((4,)),
    ]
    return pl.pallas_call(
        kernel,
        out_shape=jax.ShapeDtypeStruct((n_tok, half), BF),
        in_specs=[
            smem,
            hbm,
            vmem,
            hbm,
            hbm,
            hbm,
            vmem,
            hbm,
            vmem,
            smem,
            hbm,
            vmem,
            hbm,
            hbm,
            vmem,
            hbm,
            vmem,
            vmem,
        ],
        out_specs=hbm,
        scratch_shapes=scratch,
        compiler_params=pltpu.CompilerParams(
            collective_id=0, has_side_effects=True, vmem_limit_bytes=62 * 1024 * 1024
        ),
    )(
        slots,
        tokens,
        norm_gain.reshape(1, -1),
        branch_outer,
        branch_gate,
        branch_input,
        conv_taps,
        query_weight,
        query_gain.reshape(1, -1),
        head_scale,
        store.reshape(n_pass * plen, width),
        store_gain.reshape(1, -1),
        key_weight,
        value_weight,
        key_gain.reshape(1, -1),
        out_weight,
        gate_logit.reshape(1, -1),
        asked,
    )


def solution(mesh):
    return jax.shard_map(
        on_device,
        mesh=mesh,
        in_specs=(
            P("st", "tp"),
            P(),
            P(None, "tp"),
            P(None, "tp"),
            P(None, "tp"),
            P(None, "tp"),
            P(None, "tp"),
            P(),
            P("tp"),
            P("st", None, None),
            P(),
            P(None, "tp"),
            P(None, "tp"),
            P(),
            P(None, "tp"),
            P("tp"),
            P("st", None),
        ),
        out_specs=P("st", "tp"),
        check_vma=False,
    )
```

time: 184 us -> 75.7 us (0.41); the launches traced: 182 us -> 75.5 us
  Pallas kernels: 0 us -> 70 us
  waiting for transfers between devices: 50.4 us -> 0 us
  matrix products: 41.1 us -> 0 us
  other arithmetic: 30.7 us -> 1.45 us
  starting transfers between devices: 22.4 us -> 0 us
  local copies, waits for them, and re-layouts: 23.5 us -> 4.01 us
  between operations: 13.8 us -> 0.04 us
    pallas_call x0 -> x1, Pallas kernels: none -> 70 us  [on_device(): pl.pallas_call(kernel, out_shape=jax.ShapeDtypeStruct((n_tok, half), BF),...]
    all_to_all x2 -> x0, waiting for transfers between devices: 49.7 us -> none  [the longest x1 49.7 us: on_device(): lax.all_to_all(jnp.take(pair_table, picked, axis=0), 'st', split_axis=0,...]
    dot_general x9 -> x0, matrix products: 41.1 us -> none  [the longest x1 8.29 us: on_device(): jnp.dot(normed, branch_gate, preferred_element_type=jnp.float32)]
    all_to_all x2 -> x0, starting transfers between devices: 22.1 us -> none  [the longest x1 12 us: on_device(): lax.all_to_all(asked, 'st', split_axis=0, concat_axis=0, tiled=True)]
    reduce_sum x7 -> x2, other arithmetic: 11.8 us -> 0.8 us  [the longest x1 0.63 us: request_tables(): jnp.sum(jnp.where(match, local[:, None], 0), axis=0).reshape(1, n_st * CAP)]
    gather x3 -> x0, local copies, waits for them, and re-layouts: 10.9 us -> none  [the longest x2 8.17 us: on_device(): jnp.take(fetched.reshape(devices * capacity, passage_rows, -1), slot_inde...]
    select_n x4 -> x2, other arithmetic: 7.88 us -> 0.04 us  [request_tables(): rows.append(jnp.where(oa == 0, near, far))]
    convert_element_type x4 -> x0, other arithmetic: 7.6 us -> none  [the longest x1 3.38 us: on_device(): queries = (norm_rows(raw_query, query_gain) * (head_scale[:, None] / math...]
  transfers between devices with their start and end apart: 4 -> 0, of which waited for: 1 -> 0; matrix products, arithmetic and copies ran while one was open for 24% -> 0% of each run, Pallas kernels for 0% -> 0%
where the time goes in v1:
time: 75.7 us; the launch traced here: 75.5 us
  Pallas kernels  70 us (92%)
  local copies, waits for them, and re-layouts  4.01 us (5%)
  other arithmetic  1.45 us (2%)
    pallas_call x1, Pallas kernels, on_device(): pl.pallas_call(kernel, out_shape=jax.ShapeDtypeStruct((n_tok, half), BF),...  70 us
    unnamed x2, local copies, waits for them, and re-layouts  3.84 us

profile of v1, /device:TPU:1, one launch (start us, length us, event | category | flops | bytes accessed | tf_op | source)
XLA Modules:
  0.0 75.5 jit_solution(7861145664494672660)
XLA Ops:
  0.0 0.8 %copy.22 = s32[16,4]{1,0:T(8,128)S(1)} copy(s32[16,4]{0,1:T(4,128)} %param.33) | data formatting | bytes 512 | tf_op args[16]
  0.8 0.1 reshape.472
  0.8 0.1 reshape.471
  1.0 0.2 convert_reduce_fusion
  1.1 0.6 select_reduce_fusion
  1.8 0.6 pad_add_fusion.slots
  2.4 70.0 %shard_map.163 = bf16[1024,1024]{1,0:T(8,128)(2,1)} custom-call(s32[3,64]{1,0:T(4,128)} %pad_add_fusion.slots, bf16[1024,1024]{1,0:T(8,128)(2,1)} %tokens.1, f32[1,2048]{1,0:T(1,128)} %bitcast.27, bf16[2048,1024]{1,0:T(8,128)(2,1)} %w_outer.1, bf16[2048,1024]{1,0:T(8,128)(2,1)} %w_gate.1, bf16[2048,1024]{1,0:T(8,128)(2,1)} %w_input.1, f32[3,1024]{1,0:T(4,128)} %taps.1, ...), custom_call_target="tpu_custom_call" | custom-call | tf_op jit(solution)/shard_map/pallas_call | solution.py:585
  72.4 3.1 %copy.25 = bf16[1024,1024]{1,0:T(8,128)(2,1)} copy(bf16[1024,1024]{1,0:T(8,128)(2,1)} %shard_map.163) | data formatting | bytes 4194304
  (4 shorter events, 0.1 us)

commit v2 on v1

--- a/solution.py
+++ b/solution.py
@@ -40,21 +40,8 @@
     return (oc * RING + ob) * CAP if group == 0 else RING * RING * CAP + (oc * RING + ob) * 3 * CAP
 
 
-PLANE = [
-    (z, y, x)
-    for z in range(RING)
-    for y in range(RING)
-    for x in range(RING)
-    if (z, y, x) != (0, 0, 0) and min(z, y, x) == 0
-]
-
-
-def rel_index(moves):
-    return (moves.get("z", 0) * RING + moves.get("y", 0)) * RING + moves.get("x", 0)
-
-
 def kernel(
-    slots,
+    ids,
     tokens,
     norm_gain,
     w_outer,
@@ -71,7 +58,6 @@
     key_gain,
     w_out,
     gate_logit,
-    asked,
     out,
     v_store,
     v_wkv,
@@ -90,8 +76,9 @@
     v_out,
     v_ask,
     s_ask,
-    v_k,
-    v_v,
+    v_put,
+    v_slots,
+    s_slots,
     *rest,
 ):
     table = [rest[f * 4 : f * 4 + 4] for f in range(3)]
@@ -153,25 +140,68 @@
         weights.append(cp)
 
     barrier = pltpu.get_barrier_semaphore()
-    for z, y, x in PLANE:
-        pl.semaphore_signal(
-            barrier, inc=1, device_id=(shifted(st, {"z": z, "y": y, "x": x}), tp), device_id_type=MESH
-        )
+    for axis in STRIDE:
+        for o in OFFS:
+            pl.semaphore_signal(barrier, inc=1, device_id=(shifted(st, {axis: o}), tp), device_id_type=MESH)
     pl.semaphore_signal(barrier, inc=1, device_id=(st, other), device_id_type=MESH)
-    pl.semaphore_wait(barrier, len(PLANE) + 1)
-
-    ask_copies = []
-    for i, (z, y, x) in enumerate(PLANE):
-        cp = pltpu.make_async_remote_copy(
-            src_ref=asked,
-            dst_ref=v_ask.at[rel_index({"z": z, "y": y, "x": x})],
-            send_sem=ask_ss.at[i],
-            recv_sem=ask_rs.at[i],
-            device_id=(shifted(st, {"z": -z, "y": -y, "x": -x}), tp),
+
+    lanes = v_put.shape[1]
+    lane = lax.broadcasted_iota(jnp.int32, (1, lanes), 1)
+    lane_owner = lane // CAP
+    lane_rank = lax.rem(lane, CAP)
+    per_block, n_blocks = ids.shape
+    v_put[...] = jnp.zeros_like(v_put)
+
+    def request(j, carry):
+        wanted, count = carry
+        for p in range(per_block):
+            number = ids[p, j]
+            owner = lax.div(number, n_pass)
+            match = lane_owner == owner
+            put = match & (count == lane_rank)
+            wanted = jnp.where(put, number - owner * n_pass, wanted)
+            count = count + match.astype(jnp.int32)
+            v_put[pl.ds(j * per_block + p, 1), :] = put.astype(jnp.int32)
+        return wanted, count
+
+    zero = jnp.zeros((1, lanes), jnp.int32)
+    wanted, _ = lax.fori_loop(0, n_blocks, request, (zero, zero), unroll=4)
+    for f in range(3):
+        v_ask[f, 0, 0] = wanted
+    me = coordinates(st)
+    them = {
+        "z": lane_owner // (RING * RING),
+        "y": lax.rem(lane_owner // RING, RING),
+        "x": lax.rem(lane_owner, RING),
+    }
+    for f in range(3):
+        oa, ob, oc = [lax.rem(me[axis] - them[axis] + RING, RING) for axis in ORDERS[f]]
+        spot = oc * RING + ob
+        near = spot * CAP + lane_rank
+        far = RING * RING * CAP + spot * 3 * CAP + (oa - 1) * CAP + lane_rank
+        spots = v_put[...] * jnp.where(oa == 0, near, far)
+        v_slots[f] = jnp.sum(spots.T, axis=0, keepdims=True)
+
+    def ask_first(f, oc):
+        return pltpu.make_async_remote_copy(
+            src_ref=v_ask.at[f, 0, 0],
+            dst_ref=v_ask.at[f, 0, oc],
+            send_sem=ask_ss.at[f, oc - 1],
+            recv_sem=ask_rs.at[f, oc - 1],
+            device_id=(shifted(st, {ORDERS[f][2]: -oc}), tp),
             device_id_type=MESH,
         )
-        cp.start()
-        ask_copies.append(cp)
+
+    def ask_second(f, ob):
+        return pltpu.make_async_remote_copy(
+            src_ref=v_ask.at[f, 0],
+            dst_ref=v_ask.at[f, ob],
+            send_sem=ask_ss.at[f, 2 + ob],
+            recv_sem=ask_rs.at[f, 2 + ob],
+            device_id=(shifted(st, {ORDERS[f][1]: -ob}), tp),
+            device_id_type=MESH,
+        )
+
     tok_remote = pltpu.make_async_remote_copy(
         src_ref=tokens,
         dst_ref=v_x.at[tp],
@@ -180,16 +210,19 @@
         device_id=(st, other),
         device_id_type=MESH,
     )
-    tok_remote.start()
-    v_ask[0] = asked[...]
 
     def a_copy(f, o, p):
+        ahead = o == 1 or (o == 2 and p < 2)
+        src = table[f][0] if o != 2 else table[f][1 if ahead else 3]
+        return a_step(f, o, p, src, 1 if ahead else 3)
+
+    def a_step(f, o, p, src, move):
         return pltpu.make_async_remote_copy(
-            src_ref=table[f][0].at[pl.ds(p * 4, 4)],
+            src_ref=src.at[pl.ds(p * 4, 4)],
             dst_ref=table[f][o].at[pl.ds(p * 4, 4)],
             send_sem=a_ss.at[f * 3 + o - 1, p],
             recv_sem=a_rs.at[f * 3 + o - 1, p],
-            device_id=(shifted(st, {ORDERS[f][0]: o}), tp),
+            device_id=(shifted(st, {ORDERS[f][0]: move}), tp),
             device_id_type=MESH,
         )
 
@@ -220,32 +253,44 @@
         table[1][0][at, 0:16, :] = k[:, 48:64]
         table[1][0][at, 16:48, :] = v[:, 0:32]
         table[2][0][at, :, :] = v[:, 32:64]
-        for o in OFFS:
+
+        @pl.when(p == 0)
+        def _():
+            pl.semaphore_wait(barrier, 3 * len(OFFS) + 1)
             for f in range(3):
-                a_copy(f, o, p).start()
+                for oc in OFFS:
+                    ask_first(f, oc).start()
+
+        for f in range(3):
+            for o in (1, 3):
+                a_step(f, o, p, table[f][0], o).start()
+
+        @pl.when(p == 0)
+        def _():
+            tok_remote.start()
+
         return carry
 
     lax.fori_loop(0, 4, kv_chunk, 0)
 
-    for cp in ask_copies:
-        cp.wait_recv()
-    ask_local = pltpu.make_async_copy(v_ask, s_ask, local_sem.at[8])
-    ask_local.start()
-    ask_local.wait()
+    for f in range(3):
+        for oc in OFFS:
+            ask_first(f, oc).wait_recv()
+    for f in range(3):
+        for ob in OFFS:
+            ask_second(f, ob).start()
 
     def pack(group):
         n = len(GROUP[group]) * CAP
         for f in range(3):
-            aa, ab, ac = ORDERS[f]
-            owners = [shifted(st, {aa: -o}) for o in GROUP[group]]
-
-            def one(t, carry, f=f, ab=ab, ac=ac, owners=owners):
+            owners = [shifted(st, {ORDERS[f][0]: -o}) for o in GROUP[group]]
+
+            def one(t, carry, f=f, owners=owners):
                 ob = t // RING
                 oc = lax.rem(t, RING)
-                rel = ob * STRIDE[ab] + oc * STRIDE[ac]
                 for j, o in enumerate(GROUP[group]):
                     for r in range(CAP):
-                        at = s_ask[rel, 0, owners[j] * CAP + r]
+                        at = s_ask[f, ob, oc, 0, owners[j] * CAP + r]
                         packed[f][group][ob, oc, j * CAP + r] = table[f][o][at]
                 return carry
 
@@ -305,11 +350,7 @@
             for oc in OFFS:
                 c_copy(f, group, oc, ob).start()
 
-    pack(0)
-    send_packed(0)
-
     tok_local.wait()
-    tok_remote.wait_recv()
 
     def norm_tok(i, c):
         at = pl.ds(i * sub, sub)
@@ -321,7 +362,27 @@
         v_n[at, pl.ds(half, half)] = (x1 * r * norm_gain[:, half:width]).astype(BF)
         return c
 
-    lax.fori_loop(0, rows_tok // sub, norm_tok, 0, unroll=2)
+    tok_remote.wait_recv()
+    n_sub = rows_tok // sub
+    lax.fori_loop(0, n_sub // 2, norm_tok, 0, unroll=2)
+
+    for f in range(3):
+        for p in range(4):
+            o = 1 if p < 2 else 3
+            a_copy(f, o, p).wait_recv()
+            a_copy(f, 2, p).start()
+    for f in range(3):
+        for ob in OFFS:
+            ask_second(f, ob).wait_recv()
+    ask_local = pltpu.make_async_copy(v_ask, s_ask, local_sem.at[8])
+    ask_local.start()
+    slots_local = pltpu.make_async_copy(v_slots, s_slots, local_sem.at[9])
+    slots_local.start()
+    ask_local.wait()
+    slots_local.wait()
+    pack(0)
+    send_packed(0)
+    lax.fori_loop(n_sub // 2, n_sub, norm_tok, 0, unroll=2)
 
     weights[0].wait()
     n_heads = v_q.shape[1]
@@ -338,9 +399,9 @@
     lax.fori_loop(0, rows_tok // chunk, query_chunk, 0)
 
     for f in range(3):
-        for o in OFFS:
-            for p in range(4):
-                a_copy(f, o, p).wait_recv()
+        for p in range(4):
+            a_copy(f, 3 if p < 2 else 1, p).wait_recv()
+            a_copy(f, 2, p).wait_recv()
     pack(1)
     send_packed(1)
 
@@ -396,31 +457,28 @@
                 for ob in range(RING):
                     c_copy(f, group, oc, ob).wait_recv()
 
-    n_blocks = v_q.shape[0]
-    per_block = 4
-
-    def attend(b, carry):
+    heads_rows = n_heads * PLEN
+    ones = jnp.ones((per_block * PLEN, HD), BF)
+
+    def attend(b):
+        keys, values = [], []
         for j in range(per_block):
-            first = final[0][slots[0, b * per_block + j]]
-            second = final[1][slots[1, b * per_block + j]]
-            third = final[2][slots[2, b * per_block + j]]
-            v_k[pl.ds(j * PLEN, 48), :] = first
-            v_k[pl.ds(j * PLEN + 48, 16), :] = second[0:16]
-            v_v[pl.ds(j * PLEN, 32), :] = second[16:48]
-            v_v[pl.ds(j * PLEN + 32, 32), :] = third
-        q = v_q[b].reshape(n_heads * PLEN, HD)
-        scores = lax.dot_general(
-            q, v_k[...], (((1,), (1,)), ((), ())), preferred_element_type=F32
-        )
+            first, second, third = [
+                final[f][s_slots[f, 0, b * per_block + j]] for f in range(3)
+            ]
+            keys += [first, second[0:16]]
+            values += [second[16:48], third]
+        keys = jnp.concatenate(keys, axis=0)
+        values = jnp.concatenate([jnp.concatenate(values, axis=0), ones], axis=1)
+        q = v_q[b].reshape(heads_rows, HD)
+        scores = lax.dot_general(q, keys, (((1,), (1,)), ((), ())), preferred_element_type=F32)
         top = jnp.max(scores, axis=-1, keepdims=True)
-        weight = jnp.exp(scores - top)
-        total = jnp.sum(weight, axis=-1, keepdims=True)
-        share = (weight / total).astype(BF)
-        value = jnp.dot(share, v_v[...], preferred_element_type=F32).astype(BF)
+        weight = jnp.exp(scores - top).astype(BF)
+        value = jnp.dot(weight, values, preferred_element_type=F32)
+        value = (value[:, :HD] / value[:, HD:]).astype(BF)
         at = pl.ds(b * PLEN, PLEN)
         for h in range(n_heads):
             v_att[at, pl.ds(h * HD, HD)] = value[h * PLEN : (h + 1) * PLEN]
-        return carry
 
     def att_copy(i):
         return pltpu.make_async_remote_copy(
@@ -436,7 +494,8 @@
 
     def attend_chunk(i, carry):
         per = n_blocks // n_chunks
-        lax.fori_loop(i * per, (i + 1) * per, attend, 0)
+        for k in range(per):
+            attend(i * per + k)
         att_copy(i).start()
         return carry
 
@@ -468,8 +527,10 @@
     for i in range(n_chunks):
         out_copy(i).wait()
         att_copy(i).wait_send()
-    for cp in ask_copies:
-        cp.wait_send()
+    for f in range(3):
+        for o in OFFS:
+            ask_first(f, o).wait_send()
+            ask_second(f, o).wait_send()
     tok_remote.wait_send()
     for f in range(3):
         for o in OFFS:
@@ -482,28 +543,6 @@
             for oc in OFFS:
                 for ob in range(RING):
                     c_copy(f, group, oc, ob).wait_send()
-
-
-def request_tables(passage_ids, n_pass, n_st):
-    flat = passage_ids.reshape(-1)
-    requests = flat.shape[0]
-    owner = flat // n_pass
-    local = flat - owner * n_pass
-    order = jnp.arange(requests, dtype=jnp.int32)
-    same = (owner[:, None] == owner[None, :]) & (order[None, :] < order[:, None])
-    rank = jnp.sum(same.astype(jnp.int32), axis=1)
-    match = (owner * CAP + rank)[:, None] == jnp.arange(n_st * CAP, dtype=jnp.int32)[None, :]
-    asked = jnp.sum(jnp.where(match, local[:, None], 0), axis=0).reshape(1, n_st * CAP)
-    me = coordinates(lax.axis_index("st"))
-    them = coordinates(owner)
-    rows = []
-    for order_f in ORDERS:
-        oa, ob, oc = [lax.rem(me[axis] - them[axis] + RING, RING) for axis in order_f]
-        spot = oc * RING + ob
-        near = spot * CAP + rank
-        far = RING * RING * CAP + spot * 3 * CAP + (oa - 1) * CAP + rank
-        rows.append(jnp.where(oa == 0, near, far))
-    return asked.astype(jnp.int32), jnp.stack(rows).astype(jnp.int32)
 
 
 def on_device(
@@ -529,7 +568,6 @@
     n_tok, half = tokens.shape
     heads = head_scale.shape[0]
     n_st = lax.axis_size("st")
-    asked, slots = request_tables(passage_ids, n_pass, n_st)
     blocks = passage_ids.shape[0]
 
     vmem = pl.BlockSpec(memory_space=pltpu.VMEM)
@@ -552,10 +590,11 @@
         pltpu.VMEM((n_tok, heads * HD), BF),
         pltpu.VMEM((n_tok, heads * HD), BF),
         pltpu.VMEM((n_tok, half), BF),
-        pltpu.VMEM((n_st, 1, n_st * CAP), jnp.int32),
-        pltpu.SMEM((n_st, 1, n_st * CAP), jnp.int32),
-        pltpu.VMEM((4 * plen, HD), BF),
-        pltpu.VMEM((4 * plen, HD), BF),
+        pltpu.VMEM((3, RING, RING, 1, n_st * CAP), jnp.int32),
+        pltpu.SMEM((3, RING, RING, 1, n_st * CAP), jnp.int32),
+        pltpu.VMEM((n_st * CAP, n_st * CAP), jnp.int32),
+        pltpu.VMEM((3, 1, n_st * CAP), jnp.int32),
+        pltpu.SMEM((3, 1, n_st * CAP), jnp.int32),
     ]
     for f in range(3):
         scratch += [pltpu.VMEM((n_pass, ROWS[f], HD), BF)] * RING
@@ -566,11 +605,11 @@
     for f in range(3):
         scratch += [pltpu.VMEM((n_st * CAP, ROWS[f], HD), BF)]
     scratch += [
-        dma((9,)),
+        dma((10,)),
         dma((4,)),
         dma((4,)),
-        dma((len(PLANE),)),
-        dma((len(PLANE),)),
+        dma((3, 6)),
+        dma((3, 6)),
         dma,
         dma,
         dma((9, 4)),
@@ -603,15 +642,14 @@
             vmem,
             hbm,
             vmem,
-            vmem,
         ],
         out_specs=hbm,
         scratch_shapes=scratch,
         compiler_params=pltpu.CompilerParams(
-            collective_id=0, has_side_effects=True, vmem_limit_bytes=62 * 1024 * 1024
+            collective_id=0, has_side_effects=True, vmem_limit_bytes=56 * 1024 * 1024
         ),
     )(
-        slots,
+        passage_ids.T,
         tokens,
         norm_gain.reshape(1, -1),
         branch_outer,
@@ -628,7 +666,6 @@
         key_gain.reshape(1, -1),
         out_weight,
         gate_logit.reshape(1, -1),
-        asked,
     )
 
 

time: 75.7 us -> 68.2 us (0.901)
  Pallas kernels: 70 us -> 64.9 us
  other arithmetic: 1.45 us -> 0 us
  local copies, waits for them, and re-layouts: 4.01 us -> 3.08 us
    pallas_call x1, Pallas kernels: 70 us -> 64.9 us  [on_device(): pl.pallas_call(kernel, out_shape=jax.ShapeDtypeStruct((n_tok, half), BF),...]
    reduce_sum x2 -> x0, other arithmetic: 0.8 us -> none  [the longest x1 0.63 us: request_tables(): jnp.sum(jnp.where(match, local[:, None], 0), axis=0).reshape(1, n_st * CAP)]
    unnamed x2 -> x1, local copies, waits for them, and re-layouts: 3.84 us -> 3.08 us
where the time goes in v2:
time: 68.2 us; the launch traced here: 68 us
  Pallas kernels  64.9 us (95%)
  local copies, waits for them, and re-layouts  3.08 us (5%)
    pallas_call x1, Pallas kernels, on_device(): pl.pallas_call(kernel, out_shape=jax.ShapeDtypeStruct((n_tok, half), BF),...  64.9 us
    unnamed x1, local copies, waits for them, and re-layouts  3.08 us

profile of v2, /device:TPU:1, one launch (start us, length us, event | category | flops | bytes accessed | tf_op | source)
XLA Modules:
  0.0 68.0 jit_solution(1656835675219566673)
XLA Ops:
  0.0 64.9 %shard_map.163 = bf16[1024,1024]{1,0:T(8,128)(2,1)} custom-call(s32[4,16]{1,0:T(4,128)} %bitcast.11, bf16[1024,1024]{1,0:T(8,128)(2,1)} %tokens.1, f32[1,2048]{1,0:T(1,128)} %bitcast.8, bf16[2048,1024]{1,0:T(8,128)(2,1)} %w_outer.1, bf16[2048,1024]{1,0:T(8,128)(2,1)} %w_gate.1, bf16[2048,1024]{1,0:T(8,128)(2,1)} %w_input.1, f32[3,1024]{1,0:T(4,128)} %taps.1, ...), custom_call_target="tpu_custom_call" | custom-call | tf_op jit(solution)/shard_map/pallas_call | solution.py:624
  64.9 3.1 %copy.19 = bf16[1024,1024]{1,0:T(8,128)(2,1)} copy(bf16[1024,1024]{1,0:T(8,128)(2,1)} %shard_map.163) | data formatting | bytes 4194304

commit v3 on v2

--- a/solution.py
+++ b/solution.py
@@ -18,9 +18,10 @@
 F32 = jnp.float32
 
 ORDERS = (("z", "y", "x"), ("y", "x", "z"), ("x", "z", "y"))
-ROWS = (48, 48, 32)
+ROWS = (40, 40, 48)
 STRIDE = {"z": RING * RING, "y": RING, "x": 1}
-GROUP = ((0,), (1, 2, 3))
+GROUP = ((0,), (1, 3), (2,))
+START = (0, RING * RING * CAP, RING * RING * CAP * 3)
 OFFS = (1, 3, 2)
 
 
@@ -37,7 +38,7 @@
 
 
 def position(group, oc, ob):
-    return (oc * RING + ob) * CAP if group == 0 else RING * RING * CAP + (oc * RING + ob) * 3 * CAP
+    return START[group] + (oc * RING + ob) * len(GROUP[group]) * CAP
 
 
 def kernel(
@@ -83,10 +84,10 @@
 ):
     table = [rest[f * 4 : f * 4 + 4] for f in range(3)]
     rest = rest[12:]
-    packed = [rest[f * 2 : f * 2 + 2] for f in range(3)]
-    rest = rest[6:]
-    relay = [rest[f * 2 : f * 2 + 2] for f in range(3)]
-    rest = rest[6:]
+    packed = [rest[f * 3 : f * 3 + 3] for f in range(3)]
+    rest = rest[9:]
+    relay = [rest[f * 3 : f * 3 + 3] for f in range(3)]
+    rest = rest[9:]
     final = rest[:3]
     (
         local_sem,
@@ -177,9 +178,12 @@
     for f in range(3):
         oa, ob, oc = [lax.rem(me[axis] - them[axis] + RING, RING) for axis in ORDERS[f]]
         spot = oc * RING + ob
-        near = spot * CAP + lane_rank
-        far = RING * RING * CAP + spot * 3 * CAP + (oa - 1) * CAP + lane_rank
-        spots = v_put[...] * jnp.where(oa == 0, near, far)
+        where = jnp.zeros_like(lane)
+        for group, members in enumerate(GROUP):
+            for j, o in enumerate(members):
+                first = START[group] + spot * (len(members) * CAP) + j * CAP
+                where = jnp.where(oa == o, first + lane_rank, where)
+        spots = v_put[...] * where
         v_slots[f] = jnp.sum(spots.T, axis=0, keepdims=True)
 
     def ask_first(f, oc):
@@ -249,10 +253,11 @@
         k = k.astype(BF).reshape(4, PLEN, HD)
         v = kv[:, HD:].astype(BF).reshape(4, PLEN, HD)
         at = pl.ds(p * 4, 4)
-        table[0][0][at, :, :] = k[:, 0:48]
-        table[1][0][at, 0:16, :] = k[:, 48:64]
-        table[1][0][at, 16:48, :] = v[:, 0:32]
-        table[2][0][at, :, :] = v[:, 32:64]
+        table[0][0][at, 0:32, :] = k[:, 0:32]
+        table[0][0][at, 32:40, :] = v[:, 48:56]
+        table[1][0][at, 0:32, :] = k[:, 32:64]
+        table[1][0][at, 32:40, :] = v[:, 56:64]
+        table[2][0][at, :, :] = v[:, 0:48]
 
         @pl.when(p == 0)
         def _():
@@ -269,16 +274,18 @@
         def _():
             tok_remote.start()
 
+        @pl.when(p == 2)
+        def _():
+            for f in range(3):
+                for oc in OFFS:
+                    ask_first(f, oc).wait_recv()
+            for f in range(3):
+                for ob in OFFS:
+                    ask_second(f, ob).start()
+
         return carry
 
     lax.fori_loop(0, 4, kv_chunk, 0)
-
-    for f in range(3):
-        for oc in OFFS:
-            ask_first(f, oc).wait_recv()
-    for f in range(3):
-        for ob in OFFS:
-            ask_second(f, ob).start()
 
     def pack(group):
         n = len(GROUP[group]) * CAP
@@ -300,7 +307,7 @@
     def b_copies(f, group, ob):
         n = len(GROUP[group]) * CAP
         to = (shifted(st, {ORDERS[f][1]: ob}), tp)
-        i = (f * 2 + group) * 3 + ob - 1
+        i = (f * 3 + group) * 3 + ob - 1
         return (
             pltpu.make_async_remote_copy(
                 src_ref=packed[f][group].at[ob, pl.ds(1, 3)],
@@ -322,7 +329,7 @@
 
     def c_copy(f, group, oc, ob):
         n = len(GROUP[group]) * CAP
-        i = ((f * 2 + group) * 3 + oc - 1) * 4 + ob
+        i = ((f * 3 + group) * 3 + oc - 1) * 4 + ob
         src = packed[f][group].at[0, oc] if ob == 0 else relay[f][group].at[ob - 1, oc - 1]
         return pltpu.make_async_remote_copy(
             src_ref=src,
@@ -364,13 +371,19 @@
 
     tok_remote.wait_recv()
     n_sub = rows_tok // sub
-    lax.fori_loop(0, n_sub // 2, norm_tok, 0, unroll=2)
-
-    for f in range(3):
-        for p in range(4):
-            o = 1 if p < 2 else 3
-            a_copy(f, o, p).wait_recv()
+    quarter = n_sub // 4
+    lax.fori_loop(0, quarter, norm_tok, 0, unroll=2)
+
+    def onward(p):
+        for f in range(3):
+            a_copy(f, 1 if p < 2 else 3, p).wait_recv()
             a_copy(f, 2, p).start()
+
+    onward(0)
+    onward(1)
+    lax.fori_loop(quarter, 2 * quarter, norm_tok, 0, unroll=2)
+    onward(2)
+    onward(3)
     for f in range(3):
         for ob in OFFS:
             ask_second(f, ob).wait_recv()
@@ -382,7 +395,17 @@
     slots_local.wait()
     pack(0)
     send_packed(0)
-    lax.fori_loop(n_sub // 2, n_sub, norm_tok, 0, unroll=2)
+    for f in range(3):
+        for p in range(4):
+            a_copy(f, 3 if p < 2 else 1, p).wait_recv()
+    pack(1)
+    send_packed(1)
+    lax.fori_loop(2 * quarter, n_sub, norm_tok, 0, unroll=2)
+    for f in range(3):
+        for p in range(4):
+            a_copy(f, 2, p).wait_recv()
+    pack(2)
+    send_packed(2)
 
     weights[0].wait()
     n_heads = v_q.shape[1]
@@ -397,13 +420,6 @@
         return c
 
     lax.fori_loop(0, rows_tok // chunk, query_chunk, 0)
-
-    for f in range(3):
-        for p in range(4):
-            a_copy(f, 3 if p < 2 else 1, p).wait_recv()
-            a_copy(f, 2, p).wait_recv()
-    pack(1)
-    send_packed(1)
 
     for cp in weights[1:4]:
         cp.wait()
@@ -428,29 +444,30 @@
 
         @pl.when(s == 0)
         def _():
-            forward(0, 1)
-            forward(0, 3)
+            for ob in OFFS:
+                forward(0, ob)
 
         @pl.when(s == 1)
-        def _():
-            forward(0, 2)
-
-        @pl.when(s == 4)
         def _():
             forward(1, 1)
             forward(1, 3)
 
-        @pl.when(s == 6)
+        @pl.when(s == 2)
         def _():
             forward(1, 2)
 
+        @pl.when(s == 4)
+        def _():
+            for ob in OFFS:
+                forward(2, ob)
+
         return carry
 
     lax.fori_loop(0, (rows_tok // tall) * cols, branch, 0)
 
     weights[4].wait()
     for f in range(3):
-        for group in range(2):
+        for group in range(len(GROUP)):
             for ob in OFFS:
                 b_copies(f, group, ob)[1].wait_recv()
             for oc in OFFS:
@@ -466,8 +483,8 @@
             first, second, third = [
                 final[f][s_slots[f, 0, b * per_block + j]] for f in range(3)
             ]
-            keys += [first, second[0:16]]
-            values += [second[16:48], third]
+            keys += [first[0:32], second[0:32]]
+            values += [third, first[32:40], second[32:40]]
         keys = jnp.concatenate(keys, axis=0)
         values = jnp.concatenate([jnp.concatenate(values, axis=0), ones], axis=1)
         q = v_q[b].reshape(heads_rows, HD)
@@ -536,7 +553,7 @@
         for o in OFFS:
             for p in range(4):
                 a_copy(f, o, p).wait_send()
-        for group in range(2):
+        for group in range(len(GROUP)):
             for ob in OFFS:
                 for cp in b_copies(f, group, ob):
                     cp.wait_send()
@@ -614,10 +631,10 @@
         dma,
         dma((9, 4)),
         dma((9, 4)),
-        dma((18, 2)),
-        dma((18, 2)),
-        dma((72,)),
-        dma((72,)),
+        dma((27, 2)),
+        dma((27, 2)),
+        dma((108,)),
+        dma((108,)),
         dma((4,)),
         dma((4,)),
     ]

time: 68.2 us -> 64.8 us (0.950)
  Pallas kernels: 64.9 us -> 61.5 us
    pallas_call x1, Pallas kernels: 64.9 us -> 61.5 us  [on_device(): pl.pallas_call(kernel, out_shape=jax.ShapeDtypeStruct((n_tok, half), BF),...]
where the time goes in v3:
time: 64.8 us; the launch traced here: 64.6 us
  Pallas kernels  61.5 us (95%)
  local copies, waits for them, and re-layouts  3.08 us (5%)
    pallas_call x1, Pallas kernels, on_device(): pl.pallas_call(kernel, out_shape=jax.ShapeDtypeStruct((n_tok, half), BF),...  61.5 us
    unnamed x1, local copies, waits for them, and re-layouts  3.08 us

profile of v3, /device:TPU:1, one launch (start us, length us, event | category | flops | bytes accessed | tf_op | source)
XLA Modules:
  0.0 64.6 jit_solution(9938466246401015893)
XLA Ops:
  0.0 61.5 %shard_map.163 = bf16[1024,1024]{1,0:T(8,128)(2,1)} custom-call(s32[4,16]{1,0:T(4,128)} %bitcast.11, bf16[1024,1024]{1,0:T(8,128)(2,1)} %tokens.1, f32[1,2048]{1,0:T(1,128)} %bitcast.8, bf16[2048,1024]{1,0:T(8,128)(2,1)} %w_outer.1, bf16[2048,1024]{1,0:T(8,128)(2,1)} %w_gate.1, bf16[2048,1024]{1,0:T(8,128)(2,1)} %w_input.1, f32[3,1024]{1,0:T(4,128)} %taps.1, ...), custom_call_target="tpu_custom_call" | custom-call | tf_op jit(solution)/shard_map/pallas_call | solution.py:641
  61.5 3.1 %copy.19 = bf16[1024,1024]{1,0:T(8,128)(2,1)} copy(bf16[1024,1024]{1,0:T(8,128)(2,1)} %shard_map.163) | data formatting | bytes 4194304

commit v4 on v3

--- a/solution.py
+++ b/solution.py
@@ -23,6 +23,8 @@
 GROUP = ((0,), (1, 3), (2,))
 START = (0, RING * RING * CAP, RING * RING * CAP * 3)
 OFFS = (1, 3, 2)
+PLACE = {0: 0, 1: 1, 3: 2, 2: 3}
+PARTS = ((0,), (1, 3), (2,))
 
 
 def coordinates(st):
@@ -38,7 +40,11 @@
 
 
 def position(group, oc, ob):
-    return START[group] + (oc * RING + ob) * len(GROUP[group]) * CAP
+    return START[group] + (oc * RING + PLACE[ob]) * len(GROUP[group]) * CAP
+
+
+def place(group, ob):
+    return (PLACE[ob] - 1) * len(GROUP[group]) * CAP
 
 
 def kernel(
@@ -76,6 +82,7 @@
     v_attp,
     v_out,
     v_ask,
+    s_near,
     s_ask,
     v_put,
     v_slots,
@@ -177,7 +184,7 @@
     }
     for f in range(3):
         oa, ob, oc = [lax.rem(me[axis] - them[axis] + RING, RING) for axis in ORDERS[f]]
-        spot = oc * RING + ob
+        spot = oc * RING + jnp.where(ob == 2, 3, jnp.where(ob == 3, 2, ob))
         where = jnp.zeros_like(lane)
         for group, members in enumerate(GROUP):
             for j, o in enumerate(members):
@@ -266,15 +273,7 @@
                 for oc in OFFS:
                     ask_first(f, oc).start()
 
-        for f in range(3):
-            for o in (1, 3):
-                a_step(f, o, p, table[f][0], o).start()
-
-        @pl.when(p == 0)
-        def _():
-            tok_remote.start()
-
-        @pl.when(p == 2)
+        @pl.when(p == 3)
         def _():
             for f in range(3):
                 for oc in OFFS:
@@ -283,57 +282,59 @@
                 for ob in OFFS:
                     ask_second(f, ob).start()
 
+        for f in range(3):
+            for o in (1, 3):
+                a_step(f, o, p, table[f][0], o).start()
+
+        @pl.when(p == 0)
+        def _():
+            tok_remote.start()
+
         return carry
 
     lax.fori_loop(0, 4, kv_chunk, 0)
 
-    def pack(group):
+    def pack(group, near):
         n = len(GROUP[group]) * CAP
         for f in range(3):
             owners = [shifted(st, {ORDERS[f][0]: -o}) for o in GROUP[group]]
 
             def one(t, carry, f=f, owners=owners):
-                ob = t // RING
+                ob = 0 if near else 1 + t // RING
                 oc = lax.rem(t, RING)
                 for j, o in enumerate(GROUP[group]):
                     for r in range(CAP):
-                        at = s_ask[f, ob, oc, 0, owners[j] * CAP + r]
+                        lane_at = owners[j] * CAP + r
+                        at = s_near[f, oc, 0, lane_at] if near else s_ask[f, ob, oc, 0, lane_at]
                         packed[f][group][ob, oc, j * CAP + r] = table[f][o][at]
                 return carry
 
-            lax.fori_loop(0, RING * RING, one, 0, unroll=2)
-            final[f][pl.ds(position(group, 0, 0), n)] = packed[f][group][0, 0]
-
-    def b_copies(f, group, ob):
-        n = len(GROUP[group]) * CAP
-        to = (shifted(st, {ORDERS[f][1]: ob}), tp)
+            lax.fori_loop(0, RING * (1 if near else RING - 1), one, 0, unroll=2)
+            if near:
+                final[f][pl.ds(position(group, 0, 0), n)] = packed[f][group][0, 0]
+
+    def b_copy(f, group, ob):
         i = (f * 3 + group) * 3 + ob - 1
-        return (
-            pltpu.make_async_remote_copy(
-                src_ref=packed[f][group].at[ob, pl.ds(1, 3)],
-                dst_ref=relay[f][group].at[ob - 1],
-                send_sem=b_ss.at[i, 0],
-                recv_sem=b_rs.at[i, 0],
-                device_id=to,
-                device_id_type=MESH,
-            ),
-            pltpu.make_async_remote_copy(
-                src_ref=packed[f][group].at[ob, 0],
-                dst_ref=final[f].at[pl.ds(position(group, 0, ob), n)],
-                send_sem=b_ss.at[i, 1],
-                recv_sem=b_rs.at[i, 1],
-                device_id=to,
-                device_id_type=MESH,
-            ),
-        )
-
-    def c_copy(f, group, oc, ob):
-        n = len(GROUP[group]) * CAP
-        i = ((f * 3 + group) * 3 + oc - 1) * 4 + ob
-        src = packed[f][group].at[0, oc] if ob == 0 else relay[f][group].at[ob - 1, oc - 1]
+        return pltpu.make_async_remote_copy(
+            src_ref=packed[f][group].at[ob],
+            dst_ref=relay[f][group].at[:, pl.ds(place(group, ob), len(GROUP[group]) * CAP)],
+            send_sem=b_ss.at[i],
+            recv_sem=b_rs.at[i],
+            device_id=(shifted(st, {ORDERS[f][1]: ob}), tp),
+            device_id_type=MESH,
+        )
+
+    def c_copy(f, group, oc, part):
+        obs = PARTS[part]
+        n = len(GROUP[group]) * CAP * len(obs)
+        i = ((f * 3 + group) * 3 + oc - 1) * 3 + part
+        if part == 0:
+            src = packed[f][group].at[0, oc]
+        else:
+            src = relay[f][group].at[oc, pl.ds(place(group, obs[0]), n)]
         return pltpu.make_async_remote_copy(
             src_ref=src,
-            dst_ref=final[f].at[pl.ds(position(group, oc, ob), n)],
+            dst_ref=final[f].at[pl.ds(position(group, oc, obs[0]), n)],
             send_sem=c_ss.at[i],
             recv_sem=c_rs.at[i],
             device_id=(shifted(st, {ORDERS[f][2]: oc}), tp),
@@ -343,19 +344,22 @@
     def send_packed(group):
         for f in range(3):
             for ob in OFFS:
-                b_copies(f, group, ob)[0].start()
-        for f in range(3):
-            for ob in OFFS:
-                b_copies(f, group, ob)[1].start()
+                b_copy(f, group, ob).start()
+
+    def send_near(group):
         for f in range(3):
             for oc in OFFS:
                 c_copy(f, group, oc, 0).start()
 
-    def forward(group, ob):
+    def forward(group, part):
+        n = len(GROUP[group]) * CAP
         for f in range(3):
-            b_copies(f, group, ob)[0].wait_recv()
+            for ob in PARTS[part]:
+                b_copy(f, group, ob).wait_recv()
             for oc in OFFS:
-                c_copy(f, group, oc, ob).start()
+                c_copy(f, group, oc, part).start()
+            for ob in PARTS[part]:
+                final[f][pl.ds(position(group, 0, ob), n)] = relay[f][group][0, pl.ds(place(group, ob), n)]
 
     tok_local.wait()
 
@@ -369,10 +373,18 @@
         v_n[at, pl.ds(half, half)] = (x1 * r * norm_gain[:, half:width]).astype(BF)
         return c
 
+    near_local = pltpu.make_async_copy(v_ask.at[:, 0], s_near, local_sem.at[8])
+    near_local.start()
+    slots_local = pltpu.make_async_copy(v_slots, s_slots, local_sem.at[9])
+    slots_local.start()
     tok_remote.wait_recv()
     n_sub = rows_tok // sub
     quarter = n_sub // 4
     lax.fori_loop(0, quarter, norm_tok, 0, unroll=2)
+    near_local.wait()
+    slots_local.wait()
+    pack(0, True)
+    send_near(0)
 
     def onward(p):
         for f in range(3):
@@ -385,27 +397,27 @@
     onward(2)
     onward(3)
     for f in range(3):
+        for p in range(4):
+            a_copy(f, 3 if p < 2 else 1, p).wait_recv()
+    pack(1, True)
+    send_near(1)
+    for f in range(3):
         for ob in OFFS:
             ask_second(f, ob).wait_recv()
-    ask_local = pltpu.make_async_copy(v_ask, s_ask, local_sem.at[8])
+    ask_local = pltpu.make_async_copy(v_ask, s_ask, local_sem.at[10])
     ask_local.start()
-    slots_local = pltpu.make_async_copy(v_slots, s_slots, local_sem.at[9])
-    slots_local.start()
     ask_local.wait()
-    slots_local.wait()
-    pack(0)
-    send_packed(0)
-    for f in range(3):
-        for p in range(4):
-            a_copy(f, 3 if p < 2 else 1, p).wait_recv()
-    pack(1)
-    send_packed(1)
+    for group in range(2):
+        pack(group, False)
+        send_packed(group)
     lax.fori_loop(2 * quarter, n_sub, norm_tok, 0, unroll=2)
     for f in range(3):
         for p in range(4):
             a_copy(f, 2, p).wait_recv()
-    pack(2)
+    pack(2, False)
     send_packed(2)
+    pack(2, True)
+    send_near(2)
 
     weights[0].wait()
     n_heads = v_q.shape[1]
@@ -444,13 +456,12 @@
 
         @pl.when(s == 0)
         def _():
-            for ob in OFFS:
-                forward(0, ob)
+            forward(0, 1)
+            forward(0, 2)
 
         @pl.when(s == 1)
         def _():
             forward(1, 1)
-            forward(1, 3)
 
         @pl.when(s == 2)
         def _():
@@ -458,8 +469,8 @@
 
         @pl.when(s == 4)
         def _():
-            for ob in OFFS:
-                forward(2, ob)
+            forward(2, 1)
+            forward(2, 2)
 
         return carry
 
@@ -468,11 +479,9 @@
     weights[4].wait()
     for f in range(3):
         for group in range(len(GROUP)):
-            for ob in OFFS:
-                b_copies(f, group, ob)[1].wait_recv()
             for oc in OFFS:
-                for ob in range(RING):
-                    c_copy(f, group, oc, ob).wait_recv()
+                for part in range(3):
+                    c_copy(f, group, oc, part).wait_recv()
 
     heads_rows = n_heads * PLEN
     ones = jnp.ones((per_block * PLEN, HD), BF)
@@ -555,11 +564,30 @@
                 a_copy(f, o, p).wait_send()
         for group in range(len(GROUP)):
             for ob in OFFS:
-                for cp in b_copies(f, group, ob):
-                    cp.wait_send()
+                b_copy(f, group, ob).wait_send()
             for oc in OFFS:
-                for ob in range(RING):
-                    c_copy(f, group, oc, ob).wait_send()
+                for part in range(3):
+                    c_copy(f, group, oc, part).wait_send()
+
+
+def settle_kernel(mixed, out, held, sems):
+    pieces = sems.shape[1]
+    rows = mixed.shape[0] // pieces
+
+    def copies(i):
+        at = pl.ds(i * rows, rows)
+        return (
+            pltpu.make_async_copy(mixed.at[at], held.at[at], sems.at[0, i]),
+            pltpu.make_async_copy(held.at[at], out.at[at], sems.at[1, i]),
+        )
+
+    for i in range(pieces):
+        copies(i)[0].start()
+    for i in range(pieces):
+        copies(i)[0].wait()
+        copies(i)[1].start()
+    for i in range(pieces):
+        copies(i)[1].wait()
 
 
 def on_device(
@@ -608,6 +636,7 @@
         pltpu.VMEM((n_tok, heads * HD), BF),
         pltpu.VMEM((n_tok, half), BF),
         pltpu.VMEM((3, RING, RING, 1, n_st * CAP), jnp.int32),
+        pltpu.SMEM((3, RING, 1, n_st * CAP), jnp.int32),
         pltpu.SMEM((3, RING, RING, 1, n_st * CAP), jnp.int32),
         pltpu.VMEM((n_st * CAP, n_st * CAP), jnp.int32),
         pltpu.VMEM((3, 1, n_st * CAP), jnp.int32),
@@ -618,11 +647,11 @@
     for f in range(3):
         scratch += [pltpu.VMEM((RING, RING, len(g) * CAP, ROWS[f], HD), BF) for g in GROUP]
     for f in range(3):
-        scratch += [pltpu.VMEM((3, 3, len(g) * CAP, ROWS[f], HD), BF) for g in GROUP]
+        scratch += [pltpu.VMEM((RING, 3 * len(g) * CAP, ROWS[f], HD), BF) for g in GROUP]
     for f in range(3):
         scratch += [pltpu.VMEM((n_st * CAP, ROWS[f], HD), BF)]
     scratch += [
-        dma((10,)),
+        dma((11,)),
         dma((4,)),
         dma((4,)),
         dma((3, 6)),
@@ -631,14 +660,14 @@
         dma,
         dma((9, 4)),
         dma((9, 4)),
-        dma((27, 2)),
-        dma((27, 2)),
-        dma((108,)),
-        dma((108,)),
+        dma((27,)),
+        dma((27,)),
+        dma((81,)),
+        dma((81,)),
         dma((4,)),
         dma((4,)),
     ]
-    return pl.pallas_call(
+    mixed = pl.pallas_call(
         kernel,
         out_shape=jax.ShapeDtypeStruct((n_tok, half), BF),
         in_specs=[
@@ -684,6 +713,15 @@
         out_weight,
         gate_logit.reshape(1, -1),
     )
+    pieces = 8
+    return pl.pallas_call(
+        settle_kernel,
+        out_shape=jax.ShapeDtypeStruct((n_tok, half), BF),
+        in_specs=[hbm],
+        out_specs=hbm,
+        scratch_shapes=[pltpu.VMEM((n_tok, half), BF), dma((2, pieces))],
+        compiler_params=pltpu.CompilerParams(vmem_limit_bytes=62 * 1024 * 1024),
+    )(mixed)
 
 
 def solution(mesh):

time: 64.8 us -> 62.1 us (0.958)
  local copies, waits for them, and re-layouts: 3.08 us -> 0 us
    unnamed x1 -> x0, local copies, waits for them, and re-layouts: 3.08 us -> none
    pallas_call x0 -> x1, Pallas kernels: none -> 2.4 us  [on_device(): pl.pallas_call(settle_kernel, out_shape=jax.ShapeDtypeStruct((n_tok, half...]
    pallas_call x1, Pallas kernels: 61.5 us -> 59.5 us  [on_device(): pl.pallas_call(kernel, out_shape=jax.ShapeDtypeStruct((n_tok, half), BF),...]
where the time goes in v4:
time: 62.1 us; the launch traced here: 61.9 us
  Pallas kernels  61.9 us (100%)
    pallas_call x1, Pallas kernels, on_device(): pl.pallas_call(kernel, out_shape=jax.ShapeDtypeStruct((n_tok, half), BF),...  59.5 us
    pallas_call x1, Pallas kernels, on_device(): pl.pallas_call(settle_kernel, out_shape=jax.ShapeDtypeStruct((n_tok, half...  2.4 us

profile of v4, /device:TPU:1, one launch (start us, length us, event | category | flops | bytes accessed | tf_op | source)
XLA Modules:
  0.0 61.9 jit_solution(4663574572180797296)
XLA Ops:
  0.0 59.5 %shard_map.163.mixed = bf16[1024,1024]{1,0:T(8,128)(2,1)} custom-call(s32[4,16]{1,0:T(4,128)} %bitcast.11, bf16[1024,1024]{1,0:T(8,128)(2,1)} %tokens.1, f32[1,2048]{1,0:T(1,128)} %bitcast.8, bf16[2048,1024]{1,0:T(8,128)(2,1)} %w_outer.1, bf16[2048,1024]{1,0:T(8,128)(2,1)} %w_gate.1, bf16[2048,1024]{1,0:T(8,128)(2,1)} %w_input.1, f32[3,1024]{1,0:T(4,128)} %taps.1, ...), custom_call_target="tpu_custom_call" | custom-call | tf_op jit(solution)/shard_map/pallas_call | solution.py:670
  59.5 2.4 %shard_map.164 = bf16[1024,1024]{1,0:T(8,128)(2,1)} custom-call(bf16[1024,1024]{1,0:T(8,128)(2,1)} %shard_map.163.mixed), custom_call_target="tpu_custom_call" | custom-call | tf_op jit(solution)/shard_map/pallas_call | solution.py:717

commit v5 on v4

--- a/solution.py
+++ b/solution.py
@@ -22,7 +22,7 @@
 STRIDE = {"z": RING * RING, "y": RING, "x": 1}
 GROUP = ((0,), (1, 3), (2,))
 START = (0, RING * RING * CAP, RING * RING * CAP * 3)
-OFFS = (1, 3, 2)
+OFFS = (2, 1, 3)
 PLACE = {0: 0, 1: 1, 3: 2, 2: 3}
 PARTS = ((0,), (1, 3), (2,))
 
@@ -456,21 +456,21 @@
 
         @pl.when(s == 0)
         def _():
+            forward(0, 2)
             forward(0, 1)
-            forward(0, 2)
 
         @pl.when(s == 1)
         def _():
-            forward(1, 1)
+            forward(1, 2)
 
         @pl.when(s == 2)
         def _():
-            forward(1, 2)
+            forward(1, 1)
 
         @pl.when(s == 4)
         def _():
+            forward(2, 2)
             forward(2, 1)
-            forward(2, 2)
 
         return carry
 
@@ -478,10 +478,22 @@
 
     weights[4].wait()
     for f in range(3):
-        for group in range(len(GROUP)):
-            for oc in OFFS:
-                for part in range(3):
-                    c_copy(f, group, oc, part).wait_recv()
+        for o in OFFS:
+            ask_first(f, o).wait_send()
+            ask_second(f, o).wait_send()
+            for p in range(4):
+                a_copy(f, o, p).wait_send()
+            for group in range(len(GROUP)):
+                b_copy(f, group, o).wait_send()
+    tok_remote.wait_send()
+    for group in range(len(GROUP)):
+        for part in range(3):
+            part = (0, 2, 1)[part]
+            arriving = [c_copy(f, group, oc, part) for f in range(3) for oc in OFFS]
+            for cp in arriving:
+                cp.wait_send()
+            for cp in arriving:
+                cp.wait_recv()
 
     heads_rows = n_heads * PLEN
     ones = jnp.ones((per_block * PLEN, HD), BF)
@@ -553,21 +565,6 @@
     for i in range(n_chunks):
         out_copy(i).wait()
         att_copy(i).wait_send()
-    for f in range(3):
-        for o in OFFS:
-            ask_first(f, o).wait_send()
-            ask_second(f, o).wait_send()
-    tok_remote.wait_send()
-    for f in range(3):
-        for o in OFFS:
-            for p in range(4):
-                a_copy(f, o, p).wait_send()
-        for group in range(len(GROUP)):
-            for ob in OFFS:
-                b_copy(f, group, ob).wait_send()
-            for oc in OFFS:
-                for part in range(3):
-                    c_copy(f, group, oc, part).wait_send()
 
 
 def settle_kernel(mixed, out, held, sems):

time: 62.1 us -> 61.5 us (level)
  no operation moved by 1% of the time
where the time goes in v5:
time: 61.5 us; the launch traced here: 61.3 us
  Pallas kernels  61.3 us (100%)
    pallas_call x1, Pallas kernels, on_device(): pl.pallas_call(kernel, out_shape=jax.ShapeDtypeStruct((n_tok, half), BF),...  58.9 us
    pallas_call x1, Pallas kernels, on_device(): pl.pallas_call(settle_kernel, out_shape=jax.ShapeDtypeStruct((n_tok, half...  2.4 us

profile of v5, /device:TPU:1, one launch (start us, length us, event | category | flops | bytes accessed | tf_op | source)
XLA Modules:
  0.0 61.3 jit_solution(1342517295424234674)
XLA Ops:
  0.0 58.9 %shard_map.163.mixed = bf16[1024,1024]{1,0:T(8,128)(2,1)} custom-call(s32[4,16]{1,0:T(4,128)} %bitcast.11, bf16[1024,1024]{1,0:T(8,128)(2,1)} %tokens.1, f32[1,2048]{1,0:T(1,128)} %bitcast.8, bf16[2048,1024]{1,0:T(8,128)(2,1)} %w_outer.1, bf16[2048,1024]{1,0:T(8,128)(2,1)} %w_gate.1, bf16[2048,1024]{1,0:T(8,128)(2,1)} %w_input.1, f32[3,1024]{1,0:T(4,128)} %taps.1, ...), custom_call_target="tpu_custom_call" | custom-call | tf_op jit(solution)/shard_map/pallas_call | solution.py:667
  58.9 2.4 %shard_map.164 = bf16[1024,1024]{1,0:T(8,128)(2,1)} custom-call(bf16[1024,1024]{1,0:T(8,128)(2,1)} %shard_map.163.mixed), custom_call_target="tpu_custom_call" | custom-call | tf_op jit(solution)/shard_map/pallas_call | solution.py:714

commit v6 on v5

--- a/solution.py
+++ b/solution.py
@@ -79,7 +79,6 @@
     v_q,
     v_conv,
     v_att,
-    v_attp,
     v_out,
     v_ask,
     s_near,
@@ -496,6 +495,8 @@
                 cp.wait_recv()
 
     heads_rows = n_heads * PLEN
+    heads_width = n_heads * HD
+    own_cols = pl.ds(pl.multiple_of(tp * heads_width, heads_width), heads_width)
     ones = jnp.ones((per_block * PLEN, HD), BF)
 
     def attend(b):
@@ -516,12 +517,12 @@
         value = (value[:, :HD] / value[:, HD:]).astype(BF)
         at = pl.ds(b * PLEN, PLEN)
         for h in range(n_heads):
-            v_att[at, pl.ds(h * HD, HD)] = value[h * PLEN : (h + 1) * PLEN]
+            v_att[at, pl.ds(pl.multiple_of(tp * heads_width + h * HD, HD), HD)] = value[h * PLEN : (h + 1) * PLEN]
 
     def att_copy(i):
         return pltpu.make_async_remote_copy(
-            src_ref=v_att.at[pl.ds(i * chunk, chunk)],
-            dst_ref=v_attp.at[pl.ds(i * chunk, chunk)],
+            src_ref=v_att.at[pl.ds(i * chunk, chunk), own_cols],
+            dst_ref=v_att.at[pl.ds(i * chunk, chunk), own_cols],
             send_sem=att_ss.at[i],
             recv_sem=att_rs.at[i],
             device_id=(st, other),
@@ -539,7 +540,6 @@
 
     lax.fori_loop(0, n_chunks, attend_chunk, 0)
 
-    mine = v_att.shape[1]
 
     def out_copy(i):
         at = pl.ds(i * chunk, chunk)
@@ -548,14 +548,7 @@
     def project(i, carry):
         at = pl.ds(pl.multiple_of(i * chunk, chunk), chunk)
         att_copy(i).wait_recv()
-        cross = jnp.dot(
-            v_att[at, :], v_wout[pl.ds(pl.multiple_of(tp * mine, mine), mine), :], preferred_element_type=F32
-        )
-        cross = cross + jnp.dot(
-            v_attp[at, :],
-            v_wout[pl.ds(pl.multiple_of(other * mine, mine), mine), :],
-            preferred_element_type=F32,
-        )
+        cross = jnp.dot(v_att[at, :], v_wout[...], preferred_element_type=F32)
         v_out[at, :] = (v_conv[at, :] + jax.nn.sigmoid(gate_logit[...]) * cross).astype(BF)
         out_copy(i).start()
         return carry
@@ -629,8 +622,7 @@
         pltpu.VMEM(out_weight.shape, BF),
         pltpu.VMEM((blocks, heads, plen, HD), BF),
         pltpu.VMEM((n_tok, half), F32),
-        pltpu.VMEM((n_tok, heads * HD), BF),
-        pltpu.VMEM((n_tok, heads * HD), BF),
+        pltpu.VMEM((n_tok, 2 * heads * HD), BF),
         pltpu.VMEM((n_tok, half), BF),
         pltpu.VMEM((3, RING, RING, 1, n_st * CAP), jnp.int32),
         pltpu.SMEM((3, RING, 1, n_st * CAP), jnp.int32),

time: 61.5 us -> 61.5 us (level)
  no operation moved by 1% of the time
where the time goes in v6:
time: 61.5 us; the launch traced here: 61.3 us
  Pallas kernels  61.3 us (100%)
    pallas_call x1, Pallas kernels, on_device(): pl.pallas_call(kernel, out_shape=jax.ShapeDtypeStruct((n_tok, half), BF),...  58.9 us
    pallas_call x1, Pallas kernels, on_device(): pl.pallas_call(settle_kernel, out_shape=jax.ShapeDtypeStruct((n_tok, half...  2.4 us

profile of v6, /device:TPU:1, one launch (start us, length us, event | category | flops | bytes accessed | tf_op | source)
XLA Modules:
  0.0 61.3 jit_solution(3153354865855788020)
XLA Ops:
  0.0 58.9 %shard_map.163.mixed = bf16[1024,1024]{1,0:T(8,128)(2,1)} custom-call(s32[4,16]{1,0:T(4,128)} %bitcast.11, bf16[1024,1024]{1,0:T(8,128)(2,1)} %tokens.1, f32[1,2048]{1,0:T(1,128)} %bitcast.8, bf16[2048,1024]{1,0:T(8,128)(2,1)} %w_outer.1, bf16[2048,1024]{1,0:T(8,128)(2,1)} %w_gate.1, bf16[2048,1024]{1,0:T(8,128)(2,1)} %w_input.1, f32[3,1024]{1,0:T(4,128)} %taps.1, ...), custom_call_target="tpu_custom_call" | custom-call | tf_op jit(solution)/shard_map/pallas_call | solution.py:659
  58.9 2.4 %shard_map.164 = bf16[1024,1024]{1,0:T(8,128)(2,1)} custom-call(bf16[1024,1024]{1,0:T(8,128)(2,1)} %shard_map.163.mixed), custom_call_target="tpu_custom_call" | custom-call | tf_op jit(solution)/shard_map/pallas_call | solution.py:706
